TPU v7x, 512 devices: a whole 4x8x8 slice. The times are simulated.
512 devices in a mesh: gr: 2 (over z_hi), sp: 32 (over z_lo, y), tp: 8 (over x, core).
Axes of the slice: x: 4, y: 8, z: 8 (z_hi: 2, z_lo: 4; z = z_hi * 4 + z_lo), core: 2. Of those that a mesh axis runs over, the one named last changes fastest.
Arguments:
- inputs: bfloat16 [16384, 2048], P(('gr', 'sp'), 'tp'), parts along dimension 0, may hold values from -6 to 6
- x_weight: bfloat16 [2048, 4096], P(None, 'tp'), may hold values from -0.125 to 0.125
- b_weight: bfloat16 [2048, 2048], P(None, 'tp'), may hold values from -0.125 to 0.125
- dt_weight: bfloat16 [2048, 128], replicated, may hold values from -0.125 to 0.125
- dt_bias: float32 [2, 64], replicated, may hold values from -2 to -1
- decay_rate: float32 [2, 64], replicated, may hold values from 0.3 to 10
- conv_x: bfloat16 [5, 4096], P(None, 'tp'), may hold values from -2.5 to 2.5
- conv_b: bfloat16 [5, 2048], P(None, 'tp'), may hold values from -2.5 to 2.5
- query_c: bfloat16 [2, 16, 128], P('gr', 'tp'), parts along dimension 0, may hold values from -6 to 6
- query_gate: bfloat16 [2, 64, 64], P('gr', 'tp'), parts along dimension 0, may hold values from -6 to 6
- read_span: int32 [2], P('gr'), parts along dimension 0, may hold values from 0 to 63
- read_gain: float32 [64, 64], P('tp'), may hold values from 0.1 to 1.9
Outputs:
- span_cache: bfloat16 [128, 2, 64, 8192], P('gr', None, 'tp', 'sp'), parts along dimension 0
- first_read: bfloat16 [2, 64, 64], P('gr', 'tp'), parts along dimension 0
There are 2 independent parts, one for each index of `gr`. A program takes and returns all parts, laid end to end along the dimension named above; an argument that names none is the same for every part. Nothing has to cross between parts.
Inputs may be any that keep to these rules, and one draw needn't show every extreme that they name: read_span holds one span index from 0 to 63.
All inputs are finite; a program needn't handle non-finite values.
Results may differ from a plain program's by a relative error of at most 0.009.
Values may be sent and summed in bfloat16 or wider, within the bound.
A program may use at most 64 MiB of HBM per device.

v0:
```python
import jax
import jax.numpy as jnp
from jax import lax
from jax.sharding import PartitionSpec as P

H = 64
P_SIZE = 64
G = 16
N = 128
KW = 5
SPAN = 128


EPSILON = 1e-06


def joined_along(blocks, dim):
    lengths = list(blocks.shape[1:])
    lengths[dim] *= blocks.shape[0]
    return jnp.moveaxis(blocks, 0, dim).reshape(lengths)


def sent_to_all(shard, axis):
    size = lax.axis_size(axis)
    return lax.all_to_all(
        jnp.broadcast_to(shard[None], (size, *shard.shape)), axis, 0, 0, tiled=True
    )


def gather_directly(shard, axis, dim):
    return joined_along(sent_to_all(shard, axis), dim)


def extended(shard, sides, width):
    for axis, dim in sides:
        size, length = (lax.axis_size(axis), shard.shape[dim])
        up = [(i, (i + 1) % size) for i in range(size - 1)]
        down = [(j, i) for i, j in up]
        last = lax.slice_in_dim(shard, length - width, length, axis=dim)
        initial = lax.slice_in_dim(shard, 0, width, axis=dim)
        before = lax.ppermute(last, axis, up)
        after = lax.ppermute(initial, axis, down)
        shard = jnp.concatenate([before, shard, after], axis=dim)
    return shard


def cut_along(shard, dim, size):
    lengths = shard.shape
    blocks = shard.reshape(*lengths[:dim], size, lengths[dim] // size, *lengths[dim + 1 :])
    return jnp.moveaxis(blocks, dim, 0)


def cut_rows(length, count):
    unit = 8 if length >= 8 * count else 1
    return [length // unit * k // count * unit for k in range(1, count)]


def exchange_in_pieces(shard, axis, pieces, split_dim, concat_dim):
    blocks = cut_along(shard, split_dim, lax.axis_size(axis))
    cut = max(range(1, max(2, blocks.ndim - 1)), key=lambda d: blocks.shape[d])
    finished = []
    for share in jnp.split(blocks, cut_rows(blocks.shape[cut], pieces), axis=cut):
        if share.size:
            finished.append(lax.all_to_all(share, axis, split_axis=0, concat_axis=0, tiled=True))
    return joined_along(jnp.concatenate(finished, axis=cut), concat_dim)


def over_copies(shard, axis):
    return sent_to_all(shard, axis).sum(axis=0)


def span_states(value_rows, key_rows, step_sizes, log_decay):
    running = jnp.cumsum(log_decay, axis=1)
    closing = running[:, -1]
    forward = jnp.exp(closing[:, None, 0] - running[:, :, 0]) * step_sizes[:, :, 0]
    backward = jnp.exp(running[:, :, 1] - log_decay[:, :, 1]) * step_sizes[:, :, 1]
    weights = jnp.stack([forward, backward], axis=2)
    states = jnp.einsum(
        "kseh,kshn,kshp->kehnp",
        weights,
        key_rows.astype(jnp.float32),
        value_rows.astype(jnp.float32),
    )
    return (states, closing)


def read_weights(span_logs, chosen):
    span_count = span_logs.shape[0]
    ahead_sum = jnp.cumsum(span_logs[:, 0], axis=0)
    behind = jnp.flip(jnp.cumsum(jnp.flip(span_logs[:, 1], 0), axis=0), 0)
    positions = jnp.arange(span_count, dtype=jnp.int32)[:, None]
    ahead_pick = lax.dynamic_slice_in_dim(ahead_sum, chosen, 1, 0)
    behind_pick = lax.dynamic_slice_in_dim(behind, chosen, 1, 0)
    before = positions <= chosen
    after = positions >= chosen
    forward = jnp.where(before, jnp.exp(jnp.where(before, ahead_pick - ahead_sum, 0.0)), 0.0)
    backward = jnp.where(after, jnp.exp(jnp.where(after, behind_pick - behind, 0.0)), 0.0)
    return jnp.stack([forward, backward], axis=1)


def per_device(
    inputs,
    x_weight,
    b_weight,
    dt_weight,
    dt_bias,
    decay_rate,
    conv_x,
    conv_b,
    query_c,
    query_gate,
    read_span,
    read_gain,
):
    tokens = inputs.shape[0]
    heads_local = x_weight.shape[1] // P_SIZE
    per_group = H // G
    tp_index = lax.axis_index("tp")
    sp_index = lax.axis_index("sp")
    dt_local = lax.dynamic_slice_in_dim(
        dt_weight.reshape(dt_weight.shape[0], 2, H), tp_index * heads_local, heads_local, 2
    )
    dt_local = dt_local.reshape(dt_weight.shape[0], 2 * heads_local)
    slab_piece = gather_directly(inputs, "tp", 1)
    x_part = jnp.dot(slab_piece, x_weight, preferred_element_type=jnp.float32)
    b_part = jnp.dot(slab_piece, b_weight, preferred_element_type=jnp.float32)
    dt_part = jnp.dot(slab_piece, dt_local, preferred_element_type=jnp.float32)
    joined = jnp.concatenate([x_part.astype(jnp.bfloat16), b_part.astype(jnp.bfloat16)], axis=1)
    reach = KW // 2
    padded = extended(joined, (("sp", 0),), reach)
    taps = jnp.concatenate([conv_x, conv_b], axis=1)
    mixed_rows = jnp.zeros(joined.shape, jnp.float32)
    for offset in range(KW):
        mixed_rows = mixed_rows + taps[offset].astype(jnp.float32) * padded[
            offset : offset + tokens
        ].astype(jnp.float32)
    mixed_rows = jax.nn.silu(mixed_rows).astype(jnp.bfloat16)
    split_at = x_weight.shape[1]
    values = mixed_rows[:, :split_at]
    key_rows = mixed_rows[:, split_at:]
    length = tokens * lax.axis_size("sp")
    bias_local = lax.dynamic_slice_in_dim(dt_bias, tp_index * heads_local, heads_local, 1)
    rate_local = lax.dynamic_slice_in_dim(decay_rate, tp_index * heads_local, heads_local, 1)
    dt_raw = dt_part.astype(jnp.bfloat16).reshape(tokens, 2, heads_local)
    step_sizes = jax.nn.softplus(dt_raw.astype(jnp.float32) + bias_local)
    log_decay = -(step_sizes * rate_local) / length
    span_count = tokens // SPAN
    value_rows = values.reshape(span_count, SPAN, heads_local, P_SIZE)
    group_keys = key_rows.reshape(span_count, SPAN, heads_local // per_group, N)
    group_keys = jnp.repeat(group_keys, per_group, axis=2)
    states, closing = span_states(
        value_rows,
        group_keys,
        step_sizes.reshape(span_count, SPAN, 2, heads_local),
        log_decay.reshape(span_count, SPAN, 2, heads_local),
    )
    local_rows = states.reshape(span_count, 2, heads_local, N * P_SIZE).astype(jnp.bfloat16)
    all_logs = gather_directly(closing, "sp", 0)
    weights = read_weights(all_logs, read_span[0])
    cache_rows = exchange_in_pieces(local_rows, "sp", 2, 3, 0)
    columns = cache_rows.shape[3] // P_SIZE
    gathered = jnp.einsum("jeh,jehx->hx", weights, cache_rows.astype(jnp.float32)).reshape(
        heads_local, columns, P_SIZE
    )
    picked = lax.dynamic_slice_in_dim(query_c[0], sp_index * columns, columns, 1)
    query_cols = jnp.repeat(picked.astype(jnp.float32), per_group, axis=0)
    partial_read = jnp.einsum("hnp,hn->hp", gathered, query_cols)
    read_total = over_copies(partial_read, "sp")
    gated_read = read_total * jax.nn.silu(query_gate[0].astype(jnp.float32))
    square_sum = over_copies(jnp.sum(gated_read * gated_read), "tp")
    mean_square = square_sum / (H * P_SIZE)
    first_read = (gated_read * lax.rsqrt(mean_square + EPSILON) * read_gain)[None].astype(
        jnp.bfloat16
    )
    return (cache_rows, first_read)


def solution(mesh):
    return jax.shard_map(
        per_device,
        mesh=mesh,
        in_specs=(
            P(("gr", "sp"), "tp"),
            P(None, "tp"),
            P(None, "tp"),
            P(),
            P(),
            P(),
            P(None, "tp"),
            P(None, "tp"),
            P("gr", "tp", None),
            P("gr", "tp", None),
            P("gr"),
            P("tp", None),
        ),
        out_specs=(P("gr", None, "tp", "sp"), P("gr", "tp", None)),
        check_vma=False,
    )
```

profile of v0, /device:TPU:1, one launch (start us, length us, event | category | flops | bytes accessed | tf_op | source)
XLA Modules:
  0.0 126.6 jit_solution(1587596752569928668)
XLA Ops:
  0.6 1.1 copy.151
  1.9 1.0 broadcast_in_dim.66
  2.9 10.3 %all-to-all-start = ((bf16[8,256,256]{1,2,0:T(8,128)(2,1)}), bf16[8,256,256]{1,2,0:T(8,128)(2,1)S(1)}, u32[]{:S(2)}, u32[]{:S(2)}) async-start(bf16[8,256,256]{1,2,0:T(8,128)(2,1)} %broadcast_in_dim.66), calls=%async_computation | async-start | bytes 2097152 | tf_op jit(solution)/shard_map/all_to_all | solution.py:25
  13.2 2.0 %copy.155 = bf16[2048,128]{0,1:T(8,128)(2,1)} copy(bf16[2048,128]{1,0:T(8,128)(2,1)} %param.15) | data formatting | bytes 1048576 | tf_op args[3]
  16.6 11.5 %all-to-all-done = bf16[8,256,256]{1,2,0:T(8,128)(2,1)S(1)} async-done(((bf16[8,256,256]{1,2,0:T(8,128)(2,1)}), bf16[8,256,256]{1,2,0:T(8,128)(2,1)S(1)}, u32[]{:S(2)}, u32[]{:S(2)}) %all-to-all-start) | async-done | bytes 1048608 | tf_op jit(solution)/shard_map/all_to_all | solution.py:25
  28.2 1.1 fusion.2
  29.3 0.7 negate_multiply_fusion
  30.5 0.7 copy.182
  31.2 0.7 copy.183
  31.8 0.7 convolution_convert_fusion.1
  33.6 1.3 %collective-permute-start = (bf16[2,768]{1,0:T(2,128)(2,1)S(1)}, bf16[2,768]{1,0:T(2,128)(2,1)S(1)}, u32[]{:S(2)}, u32[]{:S(2)}) collective-permute-start(bf16[2,768]{1,0:T(2,128)(2,1)S(1)} %get-tuple-element.13), channel_id=1, source_target_pairs={{0,8},{8,16},{16,24},{24,32},{32,40},{40,48},{48,56},{56,64},{64,7... | collective-permute-start | bytes 9224 | tf_op jit(solution)/shard_map/ppermute | solution.py:41
  34.9 1.3 %collective-permute-start.1 = (bf16[2,768]{1,0:T(2,128)(2,1)S(1)}, bf16[2,768]{1,0:T(2,128)(2,1)S(1)}, u32[]{:S(2)}, u32[]{:S(2)}) collective-permute-start(bf16[2,768]{1,0:T(2,128)(2,1)S(1)} %get-tuple-element.14), channel_id=1, source_target_pairs={{8,0},{16,8},{24,16},{32,24},{40,32},{48,40},{56,48},{64,56},{72,6... | collective-permute-start | bytes 9224 | tf_op jit(solution)/shard_map/ppermute | solution.py:42
  37.0 12.1 %all-to-all-start.3 = ((f32[32,2,2,8]{3,1,2,0:T(2,128)}), f32[32,2,2,8]{3,1,2,0:T(2,128)}, u32[]{:S(2)}, u32[]{:S(2)}) async-start(f32[32,2,2,8]{3,1,2,0:T(2,128)} %broadcast_in_dim.69), calls=%async_computation.3 | async-start | bytes 131072 | tf_op jit(solution)/shard_map/all_to_all | solution.py:25
  49.3 1.3 %multiply_convert_fusion = bf16[256,768]{1,0:T(8,128)(2,1)S(1)} fusion(bf16[256,256]{1,0:T(8,128)(2,1)S(1)} %convolution_convert_fusion.2, bf16[256,512]{1,0:T(8,128)(2,1)S(1)} %convolution_convert_fusion.1, bf16[258,768]{1,0:T(8,128)(2,1)S(1)} %get-tuple-element.12, bf16[258,768]{1,0:T(8,128)(2,1)S(1)} %get-tuple-element.11, f32[768]{0:T(1024)} %get-tuple-element.3, ...), kind=kLoop, calls=%fused_computation.8 | loop fusion | flops 4325376 | bytes 2374656 | tf_op jit(solution)/shard_map/convert_element_type | solution.py:137
  50.6 0.9 slice_convert_fusion
  51.5 1.3 %reshape.171 = f32[2,128,8,64]{3,2,1,0:T(8,128)S(1)} reshape(f32[256,512]{1,0:T(8,128)} %slice_convert_fusion) | data formatting | bytes 1048576 | tf_op jit(solution)/shard_map/convert.7
  52.8 1.2 copy.154
  54.1 2.1 %fusion = bf16[2,2,8,128,64]{3,4,1,2,0:T(8,128)(2,1)} fusion(bf16[2,128,8,128,1]{3,1,4,2,0:T(8,128)(2,1)S(1)} %bitcast.85, f32[2,128,8,2]{1,3,2,0:T(2,128)S(1)} %copy.160, f32[2,128,8,64]{1,3,2,0:T(8,128)} %copy.154), kind=kOutput, calls=%fused_computation.1 | convolution fusion | flops 67633152 | bytes 1589248 | tf_op jit(solution)/shard_map/kseh,kshn,kshp->kehnp/dot_general | solution.py:78
  56.2 1.5 %copy.162 = bf16[2,2,8,128,64]{4,3,2,1,0:T(8,128)(2,1)S(1)} copy(bf16[2,2,8,128,64]{3,4,1,2,0:T(8,128)(2,1)} %fusion) | data formatting | bytes 1048576 | tf_op jit(solution)/shard_map/convert_element_type | solution.py:157
  57.8 1.5 %convert_element_type.94 = bf16[2,2,8,32,256]{4,3,2,1,0:T(8,128)(2,1)} reshape(bf16[2,2,8,128,64]{4,3,2,1,0:T(8,128)(2,1)S(1)} %copy.162) | data formatting | bytes 1048576 | tf_op jit(solution)/shard_map/convert_element_type | solution.py:157
  59.2 1.1 fusion.32
  60.3 0.9 copy.163
  61.2 9.5 %all-to-all-start.1 = ((bf16[32,2,2,4,256]{4,3,2,1,0:T(4,128)(2,1)}), bf16[32,2,2,4,256]{4,3,2,1,0:T(4,128)(2,1)S(1)}, u32[]{:S(2)}, u32[]{:S(2)}) async-start(bf16[32,2,2,4,256]{4,3,2,1,0:T(4,128)(2,1)} %copy.163), calls=%async_computation.1 | async-start | bytes 524288 | tf_op jit(solution)/shard_map/all_to_all | solution.py:64
  70.8 0.9 copy.164
  71.7 0.9 copy.166
  72.8 7.8 %all-to-all-done.1 = bf16[32,2,2,4,256]{4,3,2,1,0:T(4,128)(2,1)S(1)} async-done(((bf16[32,2,2,4,256]{4,3,2,1,0:T(4,128)(2,1)}), bf16[32,2,2,4,256]{4,3,2,1,0:T(4,128)(2,1)S(1)}, u32[]{:S(2)}, u32[]{:S(2)}) %all-to-all-start.1) | async-done | bytes 262176 | tf_op jit(solution)/shard_map/all_to_all | solution.py:64
  80.5 4.2 %all-to-all-start.2 = ((bf16[32,2,2,4,256]{4,3,2,1,0:T(4,128)(2,1)}), bf16[32,2,2,4,256]{4,3,2,1,0:T(4,128)(2,1)S(1)}, u32[]{:S(2)}, u32[]{:S(2)}) async-start(bf16[32,2,2,4,256]{4,3,2,1,0:T(4,128)(2,1)} %copy.164), calls=%async_computation.2 | async-start | bytes 524288 | tf_op jit(solution)/shard_map/all_to_all | solution.py:64
  85.2 9.3 %all-to-all-done.2 = bf16[32,2,2,4,256]{4,3,2,1,0:T(4,128)(2,1)S(1)} async-done(((bf16[32,2,2,4,256]{4,3,2,1,0:T(4,128)(2,1)}), bf16[32,2,2,4,256]{4,3,2,1,0:T(4,128)(2,1)S(1)}, u32[]{:S(2)}, u32[]{:S(2)}) %all-to-all-start.2) | async-done | bytes 262176 | tf_op jit(solution)/shard_map/all_to_all | solution.py:64
  95.4 13.2 %all_to_all.31 = f32[32,1,512]{2,1,0:T(1,128)S(1)} all-to-all(f32[32,1,512]{2,1,0:T(1,128)S(1)} %reshape.178), channel_id=1, replica_groups=mesh['gr'=2,'sp'=32,'tp'=8] {'sp'}, dimensions={0} | all-to-all | bytes 131072 | tf_op jit(solution)/shard_map/all_to_all | solution.py:25
  109.2 0.8 reduce.11
  110.7 0.6 broadcast_in_dim.75
  111.4 13.3 %all_to_all.32 = f32[8,1,1]{2,1,0:T(1,128)S(1)} all-to-all(f32[8,1,1]{2,1,0:T(1,128)S(1)} %broadcast_in_dim.75), channel_id=1, replica_groups=mesh['gr'=2,'sp'=32,'tp'=8] {'tp'}, dimensions={0} | all-to-all | bytes 64 | tf_op jit(solution)/shard_map/all_to_all | solution.py:25
  (87 shorter events, 7.3 us)
Async XLA Ops:
  0.6 31.2 %copy-start = (bf16[2048,512]{1,0:T(8,128)(2,1)S(1)}, bf16[2048,512]{1,0:T(8,128)(2,1)}, u32[]{:S(2)}) copy-start(bf16[2048,512]{1,0:T(8,128)(2,1)} %param.13) | copy-start | bytes 6291460
  1.8 14.1 %copy-start.13 = (f32[2,64]{1,0:T(2,128)S(1)}, f32[2,64]{1,0:T(2,128)}, u32[]{:S(2)}) copy-start(f32[2,64]{1,0:T(2,128)} %param.17) | copy-start | bytes 1540
  1.8 14.1 %copy-start.14 = (f32[2,64]{1,0:T(2,128)S(1)}, f32[2,64]{1,0:T(2,128)}, u32[]{:S(2)}) copy-start(f32[2,64]{1,0:T(2,128)} %param.16) | copy-start | bytes 1540
  1.8 14.2 %copy-start.10 = (bf16[5,512]{1,0:T(8,128)(2,1)S(1)}, bf16[5,512]{1,0:T(8,128)(2,1)}, u32[]{:S(2)}) copy-start(bf16[5,512]{1,0:T(8,128)(2,1)} %param.18) | copy-start | bytes 15364
  1.8 14.2 %copy-start.12 = (bf16[5,256]{1,0:T(8,128)(2,1)S(1)}, bf16[5,256]{1,0:T(8,128)(2,1)}, u32[]{:S(2)}) copy-start(bf16[5,256]{1,0:T(8,128)(2,1)} %param.19) | copy-start | bytes 7684
  2.9 25.3 %all-to-all-start = ((bf16[8,256,256]{1,2,0:T(8,128)(2,1)}), bf16[8,256,256]{1,2,0:T(8,128)(2,1)S(1)}, u32[]{:S(2)}, u32[]{:S(2)}) async-start(bf16[8,256,256]{1,2,0:T(8,128)(2,1)} %broadcast_in_dim.66), calls=%async_computation | async-start | bytes 2097152 | tf_op jit(solution)/shard_map/all_to_all | solution.py:25
  30.5 1.3 %copy-start.7 = (f32[2,2,8]{2,1,0:T(2,128)}, f32[2,2,8]{2,1,0:T(2,128)S(1)}, u32[]{:S(2)}) copy-start(f32[2,2,8]{2,1,0:T(2,128)S(1)} %slice_bitcast_fusion.2) | copy-start | bytes 388
  31.8 1.2 copy-start.2
  33.1 3.1 %copy-start.4 = (f32[2,128,2,8]{1,3,2,0:T(8,128)S(1)}, f32[2,128,2,8]{1,3,2,0:T(8,128)}, u32[]{:S(2)}) copy-start(f32[2,128,2,8]{1,3,2,0:T(8,128)} %get-tuple-element.8) | copy-start | bytes 49156
  33.1 3.1 %copy-start.5 = (f32[2,128,1,8]{1,3,2,0:T(8,128)S(1)}, f32[2,128,1,8]{1,3,2,0:T(8,128)}, u32[]{:S(2)}) copy-start(f32[2,128,1,8]{1,3,2,0:T(8,128)} %copy.182) | copy-start | bytes 24580
  33.1 3.1 %copy-start.6 = (f32[2,128,1,8]{1,3,2,0:T(8,128)S(1)}, f32[2,128,1,8]{1,3,2,0:T(8,128)}, u32[]{:S(2)}) copy-start(f32[2,128,1,8]{1,3,2,0:T(8,128)} %copy.183) | copy-start | bytes 24580
  33.1 3.2 %slice-start.1 = ((f32[2,2,8]{2,1,0:T(2,128)}), f32[2,1,8]{2,1,0:T(1,128)S(1)}, s32[]{:S(2)}) async-start(f32[2,2,8]{2,1,0:T(2,128)} %copy-done.7), calls=%async_computation.7 | async-start | bytes 2048 | tf_op jit(solution)/shard_map/slice | solution.py:75
  33.1 3.2 %copy-start.8 = (f32[2,2,8]{2,1,0:T(2,128)S(1)}, f32[2,2,8]{2,1,0:T(2,128)}, u32[]{:S(2)}) copy-start(f32[2,2,8]{2,1,0:T(2,128)} %copy-done.7) | copy-start | bytes 388
  33.6 15.5 %collective-permute-start = (bf16[2,768]{1,0:T(2,128)(2,1)S(1)}, bf16[2,768]{1,0:T(2,128)(2,1)S(1)}, u32[]{:S(2)}, u32[]{:S(2)}) collective-permute-start(bf16[2,768]{1,0:T(2,128)(2,1)S(1)} %get-tuple-element.13), channel_id=1, source_target_pairs={{0,8},{8,16},{16,24},{24,32},{32,40},{40,48},{48,56},{56,64},{64,7... | collective-permute-start | bytes 9224 | tf_op jit(solution)/shard_map/ppermute | solution.py:41
  34.9 14.2 %collective-permute-start.1 = (bf16[2,768]{1,0:T(2,128)(2,1)S(1)}, bf16[2,768]{1,0:T(2,128)(2,1)S(1)}, u32[]{:S(2)}, u32[]{:S(2)}) collective-permute-start(bf16[2,768]{1,0:T(2,128)(2,1)S(1)} %get-tuple-element.14), channel_id=1, source_target_pairs={{8,0},{16,8},{24,16},{32,24},{40,32},{48,40},{56,48},{64,56},{72,6... | collective-permute-start | bytes 9224 | tf_op jit(solution)/shard_map/ppermute | solution.py:42
  37.0 24.2 %all-to-all-start.3 = ((f32[32,2,2,8]{3,1,2,0:T(2,128)}), f32[32,2,2,8]{3,1,2,0:T(2,128)}, u32[]{:S(2)}, u32[]{:S(2)}) async-start(f32[32,2,2,8]{3,1,2,0:T(2,128)} %broadcast_in_dim.69), calls=%async_computation.3 | async-start | bytes 131072 | tf_op jit(solution)/shard_map/all_to_all | solution.py:25
  50.6 0.9 copy-start.1
  51.5 2.4 %slice-start = ((bf16[256,768]{1,0:T(8,128)(2,1)}), bf16[256,256]{1,0:T(8,128)(2,1)S(1)}, s32[]{:S(2)}) async-start(bf16[256,768]{1,0:T(8,128)(2,1)} %copy-done.1), calls=%async_computation.6 | async-start | bytes 262144 | tf_op jit(solution)/shard_map/slice | solution.py:140
  57.8 13.0 %copy-start.15 = (bf16[1,2,128]{2,1,0:T(2,128)(2,1)S(1)}, bf16[1,2,128]{2,1,0:T(2,128)(2,1)}, u32[]{:S(2)}) copy-start(bf16[1,2,128]{2,1,0:T(2,128)(2,1)} %param.20) | copy-start | bytes 1540
  61.2 19.3 %all-to-all-start.1 = ((bf16[32,2,2,4,256]{4,3,2,1,0:T(4,128)(2,1)}), bf16[32,2,2,4,256]{4,3,2,1,0:T(4,128)(2,1)S(1)}, u32[]{:S(2)}, u32[]{:S(2)}) async-start(bf16[32,2,2,4,256]{4,3,2,1,0:T(4,128)(2,1)} %copy.163), calls=%async_computation.1 | async-start | bytes 524288 | tf_op jit(solution)/shard_map/all_to_all | solution.py:64
  70.8 39.3 %copy-start.9 = (bf16[1,8,64]{2,1,0:T(8,128)(2,1)S(1)}, bf16[1,8,64]{2,1,0:T(8,128)(2,1)}, u32[]{:S(2)}) copy-start(bf16[1,8,64]{2,1,0:T(8,128)(2,1)} %param.21) | copy-start | bytes 3076
  70.8 55.2 %copy-start.11 = (f32[8,64]{1,0:T(8,128)S(1)}, f32[8,64]{1,0:T(8,128)}, u32[]{:S(2)}) copy-start(f32[8,64]{1,0:T(8,128)} %param.23) | copy-start | bytes 6148
  80.5 14.0 %all-to-all-start.2 = ((bf16[32,2,2,4,256]{4,3,2,1,0:T(4,128)(2,1)}), bf16[32,2,2,4,256]{4,3,2,1,0:T(4,128)(2,1)S(1)}, u32[]{:S(2)}, u32[]{:S(2)}) async-start(bf16[32,2,2,4,256]{4,3,2,1,0:T(4,128)(2,1)} %copy.164), calls=%async_computation.2 | async-start | bytes 524288 | tf_op jit(solution)/shard_map/all_to_all | solution.py:64
  94.8 31.9 %copy-start.3 = (bf16[32,2,2,8,256]{4,3,2,1,0:T(8,128)(2,1)}, bf16[32,2,2,8,256]{4,3,2,1,0:T(8,128)(2,1)S(1)}, u32[]{:S(2)}) copy-start(bf16[32,2,2,8,256]{4,3,2,1,0:T(8,128)(2,1)S(1)} %pad_maximum_fusion.1) | copy-start | bytes 1572868
where the time goes:
time: 128 us; the launch traced here: 127 us
  starting transfers between devices  38.7 us (30%)
  waiting for transfers between devices  28.6 us (22%)
  blocking collectives  26.6 us (21%)
  local copies, waits for them, and re-layouts  18.2 us (14%)
  other arithmetic  7.28 us (6%)
  matrix products  4.82 us (4%)
  between operations  2.43 us (2%)
    all_to_all x2, blocking collectives, sent_to_all(): lax.all_to_all(jnp.broadcast_to(shard[None], (size, *shard.shape)), axis,...  26.6 us
    all_to_all x2, starting transfers between devices, sent_to_all(): lax.all_to_all(jnp.broadcast_to(shard[None], (size, *shard.shape)), axis,...  22.4 us
    all_to_all x2, waiting for transfers between devices, exchange_in_pieces(): lax.all_to_all(share, axis, split_axis=0, concat_axis=0, tiled=True)  17.1 us
    all_to_all x2, starting transfers between devices, exchange_in_pieces(): lax.all_to_all(share, axis, split_axis=0, concat_axis=0, tiled=True)  13.7 us
    all_to_all x2, waiting for transfers between devices, sent_to_all(): lax.all_to_all(jnp.broadcast_to(shard[None], (size, *shard.shape)), axis,...  11.5 us
    unnamed x39, local copies, waits for them, and re-layouts  5.3 us
    convert_element_type x2, local copies, waits for them, and re-layouts, per_device(): states.reshape(span_count, 2, heads_local, N * P_SIZE).astype(jnp.bfloat16)  2.98 us
    split x3, local copies, waits for them, and re-layouts, exchange_in_pieces(): jnp.split(blocks, cut_rows(blocks.shape[cut], pieces), axis=cut)  2.88 us
  transfers between devices with their start and end apart: 6, of which 3 were waited for; matrix products, arithmetic and copies ran while one was open for 14% of the time, Pallas kernels for 0%

commit v1 on v0

v1 whole, which is shorter than its diff:
```python
import functools
import jax
import jax.numpy as jnp
from jax import lax
from jax.experimental import pallas as pl
from jax.experimental.pallas import tpu as pltpu
from jax.sharding import PartitionSpec as P

H = 64
P_SIZE = 64
G = 16
N = 128
KW = 5
SPAN = 128
EPSILON = 1e-06
LEN = 8192
NY = 8
NZ = 4
NX = 4
NSP = 32
NTP = 8
TOK = 256
FEAT = 256
XC = 512
BC = 256
CC = 768
WC = 896
CH = 2
CROWS = TOK // CH

MESH = pl.DeviceIdType.MESH
F32 = jnp.float32
BF16 = jnp.bfloat16


def iota(shape, dim):
    return lax.broadcasted_iota(jnp.int32, shape, dim)


def kernel(
    inputs, x_weight, b_weight, dt_weight, dt_bias, decay_rate, conv_x, conv_b,
    query_c, query_gate, read_span, read_gain,
    cache, first_read,
    slab, wbuf, acc, proj, mixed, biasb, rateb, cxb, cbb, qb, gateb, gainb, rb,
    closings, expand, sbuf, sendb, ybuf, redy, redz, reds, tot8,
    in_sem, load_sems, gsend, grecv, hsend, hrecv, csend, crecv, asend, arecv,
    ysend, yrecv, zsend, zrecv, ssend, srecv, own_sem, fsem,
):
    sp = lax.axis_index("sp")
    tp = lax.axis_index("tp")
    y = sp % NY
    z = sp // NY
    x = tp // 2
    core = tp % 2
    partner = 2 * x + 1 - core
    right = 2 * ((x + 1) % NX) + core
    left = 2 * ((x + NX - 1) % NX) + core
    across = 2 * ((x + 2) % NX) + core

    own_in = pltpu.make_async_copy(inputs, slab.at[tp], in_sem)
    own_in.start()
    loads = [
        (x_weight, wbuf.at[:, pl.ds(0, XC)]),
        (b_weight, wbuf.at[:, pl.ds(XC, BC)]),
        (dt_weight, wbuf.at[:, pl.ds(CC, 128)]),
        (dt_bias, biasb),
        (decay_rate, rateb),
        (conv_x, cxb),
        (conv_b, cbb),
        (query_c, qb),
        (query_gate, gateb),
        (read_gain, gainb),
        (read_span, rb),
    ]
    copies = []
    for i, (src, dst) in enumerate(loads):
        c = pltpu.make_async_copy(src, dst, load_sems.at[i])
        c.start()
        copies.append(c)

    barrier = pltpu.get_barrier_semaphore()

    def greet_tp(i, carry):
        pl.semaphore_signal(
            barrier, inc=1, device_id={"tp": (tp + i) % NTP}, device_id_type=MESH
        )
        return carry

    def greet_sp(i, carry):
        pl.semaphore_signal(
            barrier, inc=1, device_id={"sp": (sp + i) % NSP}, device_id_type=MESH
        )
        return carry

    lax.fori_loop(1, NTP, greet_tp, 0)
    lax.fori_loop(1, NSP, greet_sp, 0)
    er = iota((256, 1024), 0) % 128
    ec = iota((256, 1024), 1)
    expand[...] = jnp.where(
        er == (ec // 512) * H + tp * 8 + (ec % 512) // P_SIZE, 1.0, 0.0
    ).astype(BF16)
    pl.semaphore_wait(barrier, NTP - 1 + NSP - 1)

    own_in.wait()

    def part(slot, j):
        return slab.at[slot, pl.ds(j * CROWS, CROWS), :]

    sent = []

    def forward(slot, j, dest, index):
        c = pltpu.make_async_remote_copy(
            src_ref=part(slot, j),
            dst_ref=part(slot, j),
            send_sem=gsend.at[index, j],
            recv_sem=grecv.at[slot, j],
            device_id={"tp": dest},
            device_id_type=MESH,
        )
        c.start()
        sent.append(c)

    def arrive(slot, j):
        pltpu.make_async_remote_copy(
            src_ref=part(slot, j),
            dst_ref=part(slot, j),
            send_sem=gsend.at[0, j],
            recv_sem=grecv.at[slot, j],
            device_id={"tp": partner},
            device_id_type=MESH,
        ).wait_recv()

    for j in range(CH):
        forward(tp, j, right, 0)
        forward(tp, j, left, 1)
        forward(tp, j, partner, 2)

    for c in copies:
        c.wait()

    def product(slot):
        rows = pl.ds(pl.multiple_of(slot * FEAT, FEAT), FEAT)
        return jnp.dot(slab[slot], wbuf[rows, :], preferred_element_type=F32)

    fwd_slot = left * (1 - core) + right * core
    oth_slot = right * (1 - core) + left * core
    fwd_dest = oth_slot
    acc[...] = product(tp)
    for j in range(CH):
        arrive(fwd_slot, j)
        forward(fwd_slot, j, fwd_dest, 3)
        forward(fwd_slot, j, partner, 4)
        arrive(oth_slot, j)
        forward(oth_slot, j, partner, 5)
    for j in range(CH):
        arrive(partner, j)
    acc[...] += product(partner)
    acc[...] += product(fwd_slot)
    acc[...] += product(oth_slot)
    for j in range(CH):
        arrive(across, j)
        forward(across, j, partner, 6)
    acc[...] += product(across)
    for other in (left, right):
        peer = other + 1 - 2 * core
        for j in range(CH):
            arrive(peer, j)
        acc[...] += product(peer)
    peer = across + 1 - 2 * core
    for j in range(CH):
        arrive(peer, j)
    last = product(peer)
    proj[pl.ds(8, TOK), :] = (acc[:, :CC] + last[:, :CC]).astype(BF16).astype(F32)
    dt_raw = (acc[:, CC:] + last[:, CC:]).astype(BF16).astype(F32)

    def edge_up():
        return pltpu.make_async_remote_copy(
            src_ref=proj.at[pl.ds(TOK, 8), :],
            dst_ref=proj.at[pl.ds(0, 8), :],
            send_sem=hsend.at[0],
            recv_sem=hrecv.at[0],
            device_id={"sp": (sp + 1) % NSP},
            device_id_type=MESH,
        )

    def edge_down():
        return pltpu.make_async_remote_copy(
            src_ref=proj.at[pl.ds(8, 8), :],
            dst_ref=proj.at[pl.ds(TOK + 8, 8), :],
            send_sem=hsend.at[1],
            recv_sem=hrecv.at[1],
            device_id={"sp": (sp + NSP - 1) % NSP},
            device_id_type=MESH,
        )

    edge_up().start()
    edge_down().start()

    bias = jnp.concatenate([biasb[0:1, :], biasb[1:2, :]], axis=1)
    rate = jnp.concatenate([rateb[0:1, :], rateb[1:2, :]], axis=1)
    v = dt_raw + bias
    step = jnp.maximum(v, 0.0) + jnp.log1p(jnp.exp(-jnp.abs(v)))
    decay = -(step * rate) / LEN
    row = iota((SPAN, SPAN), 0)
    col = iota((SPAN, SPAN), 1)
    later = jnp.where(col > row, 1.0, 0.0)
    earlier = jnp.where(col < row, 1.0, 0.0)
    ws = []
    for k in range(2):
        a = decay[k * SPAN : (k + 1) * SPAN]
        tail = jnp.dot(later, a, precision=lax.Precision.HIGHEST, preferred_element_type=F32)
        head = jnp.dot(earlier, a, precision=lax.Precision.HIGHEST, preferred_element_type=F32)
        w = jnp.exp(jnp.where(col < H, tail, head)) * step[k * SPAN : (k + 1) * SPAN]
        closings[sp, k : k + 1, :] = jnp.sum(a, axis=0, keepdims=True)
        ws.append(w)

    def closing_copy(d, s):
        return pltpu.make_async_remote_copy(
            src_ref=closings.at[s],
            dst_ref=closings.at[s],
            send_sem=csend.at[d],
            recv_sem=crecv.at[s],
            device_id={"sp": d},
            device_id_type=MESH,
        )

    def send_closing(i, carry):
        closing_copy((sp + i) % NSP, sp).start()
        return carry

    lax.fori_loop(1, NSP, send_closing, 0)

    w = jnp.concatenate(ws, axis=0)
    w_high = w.astype(BF16)
    w_low = (w - w_high.astype(F32)).astype(BF16)
    pair = jnp.concatenate([w_high, w_low], axis=1)

    taps = [cxb[...].astype(F32), cbb[...].astype(F32)]

    def convolve(start, count):
        for block in range(CC // 256):
            tap = taps[0][:, block * 256 : (block + 1) * 256] if block < 2 else taps[1]
            cols = pl.ds(block * 256, 256)
            total = jnp.zeros((count, 256), F32)
            for o in range(KW):
                total = total + tap[o : o + 1] * proj[pl.ds(start + 6 + o, count), cols]
            mixed[pl.ds(start, count), cols] = jax.nn.silu(total).astype(BF16)

    for start in range(16, TOK - 16, 32):
        convolve(start, 32)

    edge_up().wait_recv()
    edge_down().wait_recv()

    @pl.when(sp == 0)
    def _():
        proj[pl.ds(0, 8), :] = jnp.zeros((8, CC), F32)

    @pl.when(sp == NSP - 1)
    def _():
        proj[pl.ds(TOK + 8, 8), :] = jnp.zeros((8, CC), F32)

    convolve(0, 16)
    convolve(TOK - 16, 16)

    order = (4 * (row % 32) + row // 32 == col)
    order_t = jnp.where(order, 1.0, 0.0).astype(BF16)
    contract_last = (((1,), (1,)), ((), ()))
    queries = []
    for g in range(2):
        q8 = jnp.broadcast_to(qb[0, g : g + 1, :].astype(F32), (8, N)).astype(BF16)
        queries.append(
            lax.dot_general(q8, order_t, contract_last, preferred_element_type=F32).astype(BF16)
        )
    half = iota((32, 128), 1) < P_SIZE

    def state_copy(d, s):
        return pltpu.make_async_remote_copy(
            src_ref=sendb.at[d],
            dst_ref=cache.at[pl.ds(2 * s, 2)],
            send_sem=asend.at[d],
            recv_sem=arecv.at[s],
            device_id={"sp": d},
            device_id_type=MESH,
        )

    for k in range(2):
        rows = pl.ds(k * SPAN, SPAN)
        keys_t = [
            lax.dot_general(
                order_t, mixed[rows, pl.ds(XC + g * N, N)], contract_last,
                preferred_element_type=F32,
            ).astype(BF16)
            for g in range(2)
        ]
        for e in range(2):
            wide = jnp.dot(
                pair[k * SPAN : (k + 1) * SPAN],
                expand[:, pl.ds(e * 512, 512)],
                preferred_element_type=F32,
            )
            weighted = (mixed[rows, pl.ds(0, XC)].astype(F32) * wide).astype(BF16)
            for g in range(2):
                state = jnp.dot(
                    keys_t[g], weighted[:, g * 256 : (g + 1) * 256], preferred_element_type=F32
                )
                rounded = state.astype(BF16)
                read = jnp.dot(queries[g], rounded, preferred_element_type=F32)
                ybuf[2 * k + e : 2 * k + e + 1, pl.ds(g * 256, 256)] = read[0:1]
                for j in range(2):
                    for a in range(2):
                        one = state[64 * a : 64 * a + 32, 128 * j : 128 * j + 128]
                        two = state[64 * a + 32 : 64 * a + 64, 128 * j : 128 * j + 128]
                        first = jnp.where(half, one, pltpu.roll(two, 64, 1))
                        second = jnp.where(half, pltpu.roll(one, 64, 1), two)
                        h = 4 * g + 2 * j
                        sbuf[a, pl.ds(h, 32, stride=8), :] = first
                        sbuf[a, pl.ds(h + 1, 32, stride=8), :] = second
            for a in range(2):
                sendb[:, k, e, :, pl.ds(a * 128, 128)] = sbuf[a].reshape(NSP, 8, 128).astype(BF16)

    own_out = pltpu.make_async_copy(sendb.at[sp], cache.at[pl.ds(2 * sp, 2)], own_sem)
    own_out.start()

    def peer_at(i):
        m = 7 - i % 8
        dy = (m % 2) * ((m + 1) // 2) + (1 - m % 2) * ((8 - m // 2) % 8)
        dz = 3 - i // 8
        return ((z + dz) % NZ) * NY + (y + dy) % NY

    def send_state(i, carry):
        state_copy(peer_at(i), sp).start()
        return carry

    lax.fori_loop(0, NSP - 1, send_state, 0)

    def closing_arrives(i, carry):
        s = (sp + i) % NSP
        closing_copy(s, s).wait_recv()
        return carry

    lax.fori_loop(1, NSP, closing_arrives, 0)
    chosen = rb[0]
    shape = (NSP, 2, 128)
    logs = closings[...]
    where_at = 2 * iota(shape, 0) + iota(shape, 1)
    forward_lane = iota(shape, 2) < H
    lane = iota((1, 128), 1)
    factors = []
    for k in range(2):
        mine = 2 * sp + k
        ahead = jnp.where(where_at > mine, jnp.where(where_at <= chosen, 1.0, 0.0), 0.0)
        behind = jnp.where(where_at >= chosen, jnp.where(where_at < mine, 1.0, 0.0), 0.0)
        picked = logs * jnp.where(forward_lane, ahead, behind)
        log_sum = jnp.sum(jnp.sum(picked, axis=0), axis=0, keepdims=True)
        at = jnp.full((1, 128), mine, jnp.int32)
        pick = jnp.full((1, 128), chosen, jnp.int32)
        live = jnp.where(
            lane < H,
            jnp.where(at <= pick, 1.0, 0.0),
            jnp.where(at >= pick, 1.0, 0.0),
        )
        factors.append(jnp.exp(log_sum) * live)
    factor = jnp.concatenate([jnp.broadcast_to(f, (8, 128)) for f in factors], axis=0)
    f_high = factor.astype(BF16)
    f_low = (factor - f_high.astype(F32)).astype(BF16)
    spread = jnp.dot(
        jnp.concatenate([f_high, f_low], axis=1), expand[...], preferred_element_type=F32
    )
    partial = jnp.zeros((1, 512), F32)
    for k in range(2):
        for e in range(2):
            partial = partial + (
                spread[8 * k : 8 * k + 1, e * 512 : (e + 1) * 512]
                * ybuf[2 * k + e : 2 * k + e + 1, :]
            )
    for i in range(4):
        redy[y, i : i + 1, :] = partial[:, i * 128 : (i + 1) * 128]

    def y_copy(d, s):
        return pltpu.make_async_remote_copy(
            src_ref=redy.at[s],
            dst_ref=redy.at[s],
            send_sem=ysend.at[d],
            recv_sem=yrecv.at[s],
            device_id={"sp": z * NY + d},
            device_id_type=MESH,
        )

    def z_copy(d, s):
        return pltpu.make_async_remote_copy(
            src_ref=redz.at[s],
            dst_ref=redz.at[s],
            send_sem=zsend.at[d],
            recv_sem=zrecv.at[s],
            device_id={"sp": d * NY + y},
            device_id_type=MESH,
        )

    def s_copy(d, s):
        return pltpu.make_async_remote_copy(
            src_ref=reds.at[s],
            dst_ref=reds.at[s],
            send_sem=ssend.at[d],
            recv_sem=srecv.at[s],
            device_id={"tp": d},
            device_id_type=MESH,
        )

    def each(copy, me, count, act):
        def body(i, carry):
            act(copy, me, (me + i) % count)
            return carry

        lax.fori_loop(1, count, body, 0)

    def start(copy, me, other):
        copy(other, me).start()

    def receive(copy, me, other):
        copy(other, other).wait_recv()

    def leave(copy, me, other):
        copy(other, me).wait_send()

    each(y_copy, y, NY, start)
    each(y_copy, y, NY, receive)
    redz[z] = jnp.sum(redy[...], axis=0)
    each(z_copy, z, NZ, start)
    each(z_copy, z, NZ, receive)
    total = jnp.sum(redz[...], axis=0)
    for h in range(8):
        tot8[h : h + 1, :] = total[h // 2 : h // 2 + 1, (h % 2) * 64 : (h % 2) * 64 + 64]
    gated = tot8[...] * jax.nn.silu(gateb[0].astype(F32))
    squares = jnp.sum(jnp.sum(gated * gated, axis=0, keepdims=True), axis=1, keepdims=True)
    reds[tp] = jnp.broadcast_to(squares, (1, 128))
    each(s_copy, tp, NTP, start)
    each(s_copy, tp, NTP, receive)
    square_sum = jnp.sum(reds[...], axis=0)[:, :64]
    scale = lax.rsqrt(square_sum / (H * P_SIZE) + EPSILON)
    tot8[...] = gated * scale * gainb[...]
    gateb[0] = tot8[...].astype(BF16)
    final = pltpu.make_async_copy(gateb, first_read, fsem)
    final.start()

    def state_arrives(i, carry):
        s = (sp + i) % NSP
        state_copy(s, s).wait_recv()
        return carry

    for c in sent:
        c.wait_send()
    edge_up().wait_send()
    edge_down().wait_send()
    each(closing_copy, sp, NSP, leave)
    each(y_copy, y, NY, leave)
    each(z_copy, z, NZ, leave)
    each(s_copy, tp, NTP, leave)
    lax.fori_loop(1, NSP, state_arrives, 0)
    each(state_copy, sp, NSP, leave)
    own_out.wait()
    final.wait()


def per_device(*args):
    dma = pltpu.SemaphoreType.DMA
    any_spec = pl.BlockSpec(memory_space=pl.ANY)
    return pl.pallas_call(
        kernel,
        out_shape=(
            jax.ShapeDtypeStruct((64, 2, 8, 256), BF16),
            jax.ShapeDtypeStruct((1, 8, 64), BF16),
        ),
        in_specs=[any_spec] * 12,
        out_specs=(any_spec, any_spec),
        scratch_shapes=[
            pltpu.VMEM((NTP, TOK, FEAT), BF16),
            pltpu.VMEM((2048, WC), BF16),
            pltpu.VMEM((TOK, WC), F32),
            pltpu.VMEM((TOK + 16, CC), F32),
            pltpu.VMEM((TOK, CC), BF16),
            pltpu.VMEM((2, H), F32),
            pltpu.VMEM((2, H), F32),
            pltpu.VMEM((KW, XC), BF16),
            pltpu.VMEM((KW, BC), BF16),
            pltpu.VMEM((1, 2, N), BF16),
            pltpu.VMEM((1, 8, P_SIZE), BF16),
            pltpu.VMEM((8, P_SIZE), F32),
            pltpu.SMEM((1,), jnp.int32),
            pltpu.VMEM((NSP, 2, 128), F32),
            pltpu.VMEM((256, 1024), BF16),
            pltpu.VMEM((2, 256, 128), F32),
            pltpu.VMEM((NSP, 2, 2, 8, 256), BF16),
            pltpu.VMEM((8, 512), F32),
            pltpu.VMEM((NY, 4, 128), F32),
            pltpu.VMEM((NZ, 4, 128), F32),
            pltpu.VMEM((NTP, 1, 128), F32),
            pltpu.VMEM((8, P_SIZE), F32),
            dma,
            dma((11,)),
            dma((7, CH)),
            dma((NTP, CH)),
            dma((2,)),
            dma((2,)),
            dma((NSP,)),
            dma((NSP,)),
            dma((NSP,)),
            dma((NSP,)),
            dma((NY,)),
            dma((NY,)),
            dma((NZ,)),
            dma((NZ,)),
            dma((NTP,)),
            dma((NTP,)),
            dma,
            dma,
        ],
        compiler_params=pltpu.CompilerParams(collective_id=0, has_side_effects=True),
    )(*args)


def solution(mesh):
    return jax.shard_map(
        per_device,
        mesh=mesh,
        in_specs=(
            P(("gr", "sp"), "tp"),
            P(None, "tp"),
            P(None, "tp"),
            P(),
            P(),
            P(),
            P(None, "tp"),
            P(None, "tp"),
            P("gr", "tp", None),
            P("gr", "tp", None),
            P("gr"),
            P("tp", None),
        ),
        out_specs=(P("gr", None, "tp", "sp"), P("gr", "tp", None)),
        check_vma=False,
    )
```

time: 128 us -> 56 us (0.44)
  Pallas kernels: 0 us -> 50.9 us
  starting transfers between devices: 38.7 us -> 0 us
  waiting for transfers between devices: 28.6 us -> 0 us
  blocking collectives: 26.6 us -> 0 us
  local copies, waits for them, and re-layouts: 18.2 us -> 3.12 us
  other arithmetic: 7.28 us -> 0 us
  matrix products: 4.82 us -> 0 us
    pallas_call x0 -> x1, Pallas kernels: none -> 50.9 us  [per_device(): pl.pallas_call(kernel, out_shape=(jax.ShapeDtypeStruct((64, 2, 8, 256), B...]
    all_to_all x4 -> x0, starting transfers between devices: 36.1 us -> none  [the longest x2 22.4 us: sent_to_all(): lax.all_to_all(jnp.broadcast_to(shard[None], (size, *shard.shape)), axis,...]
    all_to_all x4 -> x0, waiting for transfers between devices: 28.6 us -> none  [the longest x2 17.1 us: exchange_in_pieces(): lax.all_to_all(share, axis, split_axis=0, concat_axis=0, tiled=True)]
    all_to_all x2 -> x0, blocking collectives: 26.6 us -> none  [sent_to_all(): lax.all_to_all(jnp.broadcast_to(shard[None], (size, *shard.shape)), axis,...]
    dot_general x6 -> x0, matrix products: 4.82 us -> none  [the longest x1 2.14 us: span_states(): jnp.einsum('kseh,kshn,kshp->kehnp', weights, key_rows.astype(jnp.float32)...]
    convert_element_type x3 -> x0, local copies, waits for them, and re-layouts: 2.99 us -> none  [the longest x2 2.98 us: per_device(): states.reshape(span_count, 2, heads_local, N * P_SIZE).astype(jnp.bfloat16)]
    split x3 -> x0, local copies, waits for them, and re-layouts: 2.88 us -> none  [exchange_in_pieces(): jnp.split(blocks, cut_rows(blocks.shape[cut], pieces), axis=cut)]
    ppermute x2 -> x0, starting transfers between devices: 2.58 us -> none  [the longest x1 1.29 us: extended(): after = lax.ppermute(initial, axis, down)]
  transfers between devices with their start and end apart: 6 -> 0, of which waited for: 3 -> 0; matrix products, arithmetic and copies ran while one was open for 14% -> 0% of each run, Pallas kernels for 0% -> 0%
where the time goes in v1:
time: 56 us; the launch traced here: 55.3 us
  Pallas kernels  50.9 us (91%)
  local copies, waits for them, and re-layouts  3.12 us (6%)
  between operations  1.29 us (2%)
    pallas_call x1, Pallas kernels, per_device(): pl.pallas_call(kernel, out_shape=(jax.ShapeDtypeStruct((64, 2, 8, 256), B...  50.9 us
    unnamed x2, local copies, waits for them, and re-layouts  3.12 us

profile of v1, /device:TPU:1, one launch (start us, length us, event | category | flops | bytes accessed | tf_op | source)
XLA Modules:
  0.0 55.3 jit_solution(15680998046383369230)
XLA Ops:
  1.3 50.9 %shard_map.131 = (bf16[64,2,8,256]{3,2,1,0:T(8,128)(2,1)}, bf16[1,8,64]{2,1,0:T(8,128)(2,1)}) custom-call(bf16[256,256]{1,0:T(8,128)(2,1)} %inputs.1, bf16[2048,512]{1,0:T(8,128)(2,1)} %x_weight.1, bf16[2048,256]{1,0:T(8,128)(2,1)} %b_weight.1, bf16[2048,128]{1,0:T(8,128)(2,1)} %dt_weight.1, f32[2,64]{1,0:T(2,128)} %dt_bias.1, f32[2,64]{1,0:T(2,128)} %decay_rate.1, ...), custom_call_target="tpu_custom_call" | custom-call | tf_op jit(solution)/shard_map/pallas_call | solution.py:468
  52.2 1.9 %copy.17 = bf16[64,2,8,256]{3,2,1,0:T(8,128)(2,1)} copy(bf16[64,2,8,256]{3,2,1,0:T(8,128)(2,1)} %get-tuple-element.4) | data formatting | bytes 1048576
  54.1 1.3 %copy.18 = bf16[1,8,64]{2,1,0:T(8,128)(2,1)} copy(bf16[1,8,64]{2,1,0:T(8,128)(2,1)} %get-tuple-element.5) | data formatting | bytes 2048

commit v2 on v1

--- a/solution.py
+++ b/solution.py
@@ -25,7 +25,8 @@
 BC = 256
 CC = 768
 WC = 896
-CH = 2
+CH = 4
+EARLY = 3
 CROWS = TOK // CH
 
 MESH = pl.DeviceIdType.MESH
@@ -42,9 +43,9 @@
     query_c, query_gate, read_span, read_gain,
     cache, first_read,
     slab, wbuf, acc, proj, mixed, biasb, rateb, cxb, cbb, qb, gateb, gainb, rb,
-    closings, expand, sbuf, sendb, ybuf, redy, redz, reds, tot8,
+    closings, blocks, expand, sbuf, sendb, ybuf, redy, redz, reds, tot8,
     in_sem, load_sems, gsend, grecv, hsend, hrecv, csend, crecv, asend, arecv,
-    ysend, yrecv, zsend, zrecv, ssend, srecv, own_sem, fsem,
+    ysend, yrecv, zsend, zrecv, usend, urecv, ssend, srecv, own_sem, stage,
 ):
     sp = lax.axis_index("sp")
     tp = lax.axis_index("tp")
@@ -80,26 +81,39 @@
 
     barrier = pltpu.get_barrier_semaphore()
 
+    def at_y(other):
+        return {"sp": z * NY + (other + NY) % NY}
+
     def greet_tp(i, carry):
         pl.semaphore_signal(
             barrier, inc=1, device_id={"tp": (tp + i) % NTP}, device_id_type=MESH
         )
         return carry
 
-    def greet_sp(i, carry):
+    def greet_z(i, carry):
         pl.semaphore_signal(
-            barrier, inc=1, device_id={"sp": (sp + i) % NSP}, device_id_type=MESH
+            barrier, inc=1, device_id={"sp": ((z + i) % NZ) * NY + y}, device_id_type=MESH
         )
         return carry
 
     lax.fori_loop(1, NTP, greet_tp, 0)
-    lax.fori_loop(1, NSP, greet_sp, 0)
+    lax.fori_loop(1, NZ, greet_z, 0)
+    for side in (1, -1):
+        pl.semaphore_signal(barrier, inc=1, device_id=at_y(y + side), device_id_type=MESH)
+
+    def tell(index, distance):
+        for side in (distance, -distance):
+            pl.semaphore_signal(
+                stage.at[index], inc=1, device_id=at_y(y + side), device_id_type=MESH
+            )
+
     er = iota((256, 1024), 0) % 128
     ec = iota((256, 1024), 1)
     expand[...] = jnp.where(
         er == (ec // 512) * H + tp * 8 + (ec % 512) // P_SIZE, 1.0, 0.0
     ).astype(BF16)
-    pl.semaphore_wait(barrier, NTP - 1 + NSP - 1)
+    pl.semaphore_wait(barrier, NTP - 1 + NZ - 1 + 2)
+    tell(0, 1)
 
     own_in.wait()
 
@@ -133,6 +147,7 @@
     for j in range(CH):
         forward(tp, j, right, 0)
         forward(tp, j, left, 1)
+    for j in range(CH):
         forward(tp, j, partner, 2)
 
     for c in copies:
@@ -152,24 +167,31 @@
         forward(fwd_slot, j, partner, 4)
         arrive(oth_slot, j)
         forward(oth_slot, j, partner, 5)
-    for j in range(CH):
-        arrive(partner, j)
-    acc[...] += product(partner)
+        if j == 0:
+            for i in range(CH):
+                arrive(partner, i)
+            acc[...] += product(partner)
+            pl.semaphore_wait(stage.at[0], 2)
+            tell(1, 2)
     acc[...] += product(fwd_slot)
+    pl.semaphore_wait(stage.at[1], 2)
+    tell(2, 1)
     acc[...] += product(oth_slot)
+    others = [left + 1 - 2 * core, right + 1 - 2 * core]
     for j in range(CH):
         arrive(across, j)
         forward(across, j, partner, 6)
+        if j % 2 == 1:
+            peer = others[j // 2]
+            for i in range(CH):
+                arrive(peer, i)
+            acc[...] += product(peer)
     acc[...] += product(across)
-    for other in (left, right):
-        peer = other + 1 - 2 * core
-        for j in range(CH):
-            arrive(peer, j)
-        acc[...] += product(peer)
     peer = across + 1 - 2 * core
     for j in range(CH):
         arrive(peer, j)
     last = product(peer)
+    pl.semaphore_wait(stage.at[2], 2)
     proj[pl.ds(8, TOK), :] = (acc[:, :CC] + last[:, :CC]).astype(BF16).astype(F32)
     dt_raw = (acc[:, CC:] + last[:, CC:]).astype(BF16).astype(F32)
 
@@ -211,24 +233,51 @@
         tail = jnp.dot(later, a, precision=lax.Precision.HIGHEST, preferred_element_type=F32)
         head = jnp.dot(earlier, a, precision=lax.Precision.HIGHEST, preferred_element_type=F32)
         w = jnp.exp(jnp.where(col < H, tail, head)) * step[k * SPAN : (k + 1) * SPAN]
-        closings[sp, k : k + 1, :] = jnp.sum(a, axis=0, keepdims=True)
+        closings[y, k : k + 1, :] = jnp.sum(a, axis=0, keepdims=True)
         ws.append(w)
 
-    def closing_copy(d, s):
-        return pltpu.make_async_remote_copy(
-            src_ref=closings.at[s],
-            dst_ref=closings.at[s],
-            send_sem=csend.at[d],
-            recv_sem=crecv.at[s],
-            device_id={"sp": d},
-            device_id_type=MESH,
-        )
-
-    def send_closing(i, carry):
-        closing_copy((sp + i) % NSP, sp).start()
-        return carry
-
-    lax.fori_loop(1, NSP, send_closing, 0)
+    def y_exchange(buffer, send_sem, recv_sem):
+        return lambda d, s: pltpu.make_async_remote_copy(
+            src_ref=buffer.at[s],
+            dst_ref=buffer.at[s],
+            send_sem=send_sem.at[d],
+            recv_sem=recv_sem.at[s],
+            device_id=at_y(d),
+            device_id_type=MESH,
+        )
+
+    def z_exchange(buffer, send_sem, recv_sem):
+        return lambda d, s: pltpu.make_async_remote_copy(
+            src_ref=buffer.at[s],
+            dst_ref=buffer.at[s],
+            send_sem=send_sem.at[d],
+            recv_sem=recv_sem.at[s],
+            device_id={"sp": d * NY + y},
+            device_id_type=MESH,
+        )
+
+    closing_copy = y_exchange(closings, csend, crecv)
+    y_copy = y_exchange(redy, ysend, yrecv)
+    z_copy = z_exchange(redz, zsend, zrecv)
+    block_copy = z_exchange(blocks, usend, urecv)
+
+    def each(copy, me, count, act):
+        def body(i, carry):
+            act(copy, me, (me + i) % count)
+            return carry
+
+        lax.fori_loop(1, count, body, 0)
+
+    def start(copy, me, other):
+        copy(other, me).start()
+
+    def receive(copy, me, other):
+        copy(other, other).wait_recv()
+
+    def leave(copy, me, other):
+        copy(other, me).wait_send()
+
+    each(closing_copy, y, NY, start)
 
     w = jnp.concatenate(ws, axis=0)
     w_high = w.astype(BF16)
@@ -246,23 +295,6 @@
                 total = total + tap[o : o + 1] * proj[pl.ds(start + 6 + o, count), cols]
             mixed[pl.ds(start, count), cols] = jax.nn.silu(total).astype(BF16)
 
-    for start in range(16, TOK - 16, 32):
-        convolve(start, 32)
-
-    edge_up().wait_recv()
-    edge_down().wait_recv()
-
-    @pl.when(sp == 0)
-    def _():
-        proj[pl.ds(0, 8), :] = jnp.zeros((8, CC), F32)
-
-    @pl.when(sp == NSP - 1)
-    def _():
-        proj[pl.ds(TOK + 8, 8), :] = jnp.zeros((8, CC), F32)
-
-    convolve(0, 16)
-    convolve(TOK - 16, 16)
-
     order = (4 * (row % 32) + row // 32 == col)
     order_t = jnp.where(order, 1.0, 0.0).astype(BF16)
     contract_last = (((1,), (1,)), ((), ()))
@@ -274,18 +306,56 @@
         )
     half = iota((32, 128), 1) < P_SIZE
 
-    def state_copy(d, s):
+    def state_copy(k, d, s):
         return pltpu.make_async_remote_copy(
-            src_ref=sendb.at[d],
-            dst_ref=cache.at[pl.ds(2 * s, 2)],
-            send_sem=asend.at[d],
-            recv_sem=arecv.at[s],
+            src_ref=sendb.at[d, k],
+            dst_ref=cache.at[2 * s + k],
+            send_sem=asend.at[k, d],
+            recv_sem=arecv.at[k, s],
             device_id={"sp": d},
             device_id_type=MESH,
         )
 
+    def send_states(k, first, last):
+        def body(i, carry):
+            m = 7 - (first + i // NZ)
+            dy = (m % 2) * ((m + 1) // 2) + (1 - m % 2) * (8 - m // 2)
+            d = ((z + i % NZ) % NZ) * NY + (y + dy) % NY
+            state_copy(k, d, sp).start()
+            return carry
+
+        lax.fori_loop(0, (last - first) * NZ, body, 0)
+
+    def send_column(k):
+        def body(i, carry):
+            state_copy(k, ((z + i) % NZ) * NY + y, sp).start()
+            return carry
+
+        lax.fori_loop(1, NZ, body, 0)
+
+    own_out = []
     for k in range(2):
         rows = pl.ds(k * SPAN, SPAN)
+        if k == 0:
+            for first in range(16, SPAN, 16):
+                convolve(first, 16)
+            edge_up().wait_recv()
+
+            @pl.when(sp == 0)
+            def _():
+                proj[pl.ds(0, 8), :] = jnp.zeros((8, CC), F32)
+
+            convolve(0, 16)
+        else:
+            for first in range(SPAN, TOK - 16, 16):
+                convolve(first, 16)
+            edge_down().wait_recv()
+
+            @pl.when(sp == NSP - 1)
+            def _():
+                proj[pl.ds(TOK + 8, 8), :] = jnp.zeros((8, CC), F32)
+
+            convolve(TOK - 16, 16)
         keys_t = [
             lax.dot_general(
                 order_t, mixed[rows, pl.ds(XC + g * N, N)], contract_last,
@@ -306,7 +376,7 @@
                 )
                 rounded = state.astype(BF16)
                 read = jnp.dot(queries[g], rounded, preferred_element_type=F32)
-                ybuf[2 * k + e : 2 * k + e + 1, pl.ds(g * 256, 256)] = read[0:1]
+                ybuf[k : k + 1, pl.ds(e * 512 + g * 256, 256)] = read[0:1]
                 for j in range(2):
                     for a in range(2):
                         one = state[64 * a : 64 * a + 32, 128 * j : 128 * j + 128]
@@ -319,40 +389,36 @@
             for a in range(2):
                 sendb[:, k, e, :, pl.ds(a * 128, 128)] = sbuf[a].reshape(NSP, 8, 128).astype(BF16)
 
-    own_out = pltpu.make_async_copy(sendb.at[sp], cache.at[pl.ds(2 * sp, 2)], own_sem)
-    own_out.start()
-
-    def peer_at(i):
-        m = 7 - i % 8
-        dy = (m % 2) * ((m + 1) // 2) + (1 - m % 2) * ((8 - m // 2) % 8)
-        dz = 3 - i // 8
-        return ((z + dz) % NZ) * NY + (y + dy) % NY
-
-    def send_state(i, carry):
-        state_copy(peer_at(i), sp).start()
-        return carry
-
-    lax.fori_loop(0, NSP - 1, send_state, 0)
-
-    def closing_arrives(i, carry):
-        s = (sp + i) % NSP
-        closing_copy(s, s).wait_recv()
-        return carry
-
-    lax.fori_loop(1, NSP, closing_arrives, 0)
+        own_out.append(
+            pltpu.make_async_copy(sendb.at[sp, k], cache.at[2 * sp + k], own_sem.at[k])
+        )
+        own_out[k].start()
+        if k == 0:
+            send_column(0)
+            send_states(0, 0, EARLY)
+
+    each(closing_copy, y, NY, receive)
     chosen = rb[0]
-    shape = (NSP, 2, 128)
+    shape = (NY, 2, 128)
     logs = closings[...]
-    where_at = 2 * iota(shape, 0) + iota(shape, 1)
+    where_at = 2 * NY * z + 2 * iota(shape, 0) + iota(shape, 1)
     forward_lane = iota(shape, 2) < H
+    up_to = jnp.where(where_at <= chosen, 1.0, 0.0)
+    on_from = jnp.where(where_at >= chosen, 1.0, 0.0)
     lane = iota((1, 128), 1)
+
+    def log_total(ahead, behind):
+        picked = logs * jnp.where(forward_lane, ahead, behind)
+        return jnp.sum(jnp.sum(picked, axis=0), axis=0, keepdims=True)
+
+    blocks[z] = log_total(up_to, on_from)
+    each(block_copy, z, NZ, start)
     factors = []
     for k in range(2):
         mine = 2 * sp + k
-        ahead = jnp.where(where_at > mine, jnp.where(where_at <= chosen, 1.0, 0.0), 0.0)
-        behind = jnp.where(where_at >= chosen, jnp.where(where_at < mine, 1.0, 0.0), 0.0)
-        picked = logs * jnp.where(forward_lane, ahead, behind)
-        log_sum = jnp.sum(jnp.sum(picked, axis=0), axis=0, keepdims=True)
+        log_sum = log_total(
+            jnp.where(where_at > mine, up_to, 0.0), jnp.where(where_at < mine, on_from, 0.0)
+        )
         at = jnp.full((1, 128), mine, jnp.int32)
         pick = jnp.full((1, 128), chosen, jnp.int32)
         live = jnp.where(
@@ -360,42 +426,36 @@
             jnp.where(at <= pick, 1.0, 0.0),
             jnp.where(at >= pick, 1.0, 0.0),
         )
-        factors.append(jnp.exp(log_sum) * live)
-    factor = jnp.concatenate([jnp.broadcast_to(f, (8, 128)) for f in factors], axis=0)
-    f_high = factor.astype(BF16)
-    f_low = (factor - f_high.astype(F32)).astype(BF16)
-    spread = jnp.dot(
-        jnp.concatenate([f_high, f_low], axis=1), expand[...], preferred_element_type=F32
-    )
-    partial = jnp.zeros((1, 512), F32)
-    for k in range(2):
-        for e in range(2):
-            partial = partial + (
-                spread[8 * k : 8 * k + 1, e * 512 : (e + 1) * 512]
-                * ybuf[2 * k + e : 2 * k + e + 1, :]
-            )
-    for i in range(4):
-        redy[y, i : i + 1, :] = partial[:, i * 128 : (i + 1) * 128]
-
-    def y_copy(d, s):
-        return pltpu.make_async_remote_copy(
-            src_ref=redy.at[s],
-            dst_ref=redy.at[s],
-            send_sem=ysend.at[d],
-            recv_sem=yrecv.at[s],
-            device_id={"sp": z * NY + d},
-            device_id_type=MESH,
-        )
-
-    def z_copy(d, s):
-        return pltpu.make_async_remote_copy(
-            src_ref=redz.at[s],
-            dst_ref=redz.at[s],
-            send_sem=zsend.at[d],
-            recv_sem=zrecv.at[s],
-            device_id={"sp": d * NY + y},
-            device_id_type=MESH,
-        )
+        factors.append(jnp.broadcast_to(jnp.exp(log_sum) * live, (8, 128)))
+
+    def spread(rows):
+        high = rows.astype(BF16)
+        low = (rows - high.astype(F32)).astype(BF16)
+        return jnp.dot(
+            jnp.concatenate([high, low], axis=1), expand[...], preferred_element_type=F32
+        )
+
+    wide_factor = spread(jnp.concatenate(factors, axis=0))
+    redy[y] = wide_factor[0:1] * ybuf[0:1, :] + wide_factor[8:9] * ybuf[1:2, :]
+    each(y_copy, y, NY, start)
+    send_states(0, EARLY, 7)
+    send_column(1)
+    send_states(1, 0, 7)
+
+    each(block_copy, z, NZ, receive)
+    block_rows = []
+    for block in range(NZ):
+        after = jnp.zeros((1, 128), F32)
+        before = jnp.zeros((1, 128), F32)
+        for other in range(block + 1, NZ):
+            after = after + blocks[other]
+        for other in range(block):
+            before = before + blocks[other]
+        block_rows.append(
+            jnp.broadcast_to(jnp.exp(jnp.where(lane < H, after, before)), (8, 128))
+        )
+    block_factor = spread(jnp.concatenate(block_rows, axis=0))
+    gate = jax.nn.silu(gateb[0].astype(F32))
 
     def s_copy(d, s):
         return pltpu.make_async_remote_copy(
@@ -407,72 +467,53 @@
             device_id_type=MESH,
         )
 
-    def each(copy, me, count, act):
-        def body(i, carry):
-            act(copy, me, (me + i) % count)
-            return carry
-
-        lax.fori_loop(1, count, body, 0)
-
-    def start(copy, me, other):
-        copy(other, me).start()
-
-    def receive(copy, me, other):
-        copy(other, other).wait_recv()
-
-    def leave(copy, me, other):
-        copy(other, me).wait_send()
-
-    each(y_copy, y, NY, start)
     each(y_copy, y, NY, receive)
     redz[z] = jnp.sum(redy[...], axis=0)
     each(z_copy, z, NZ, start)
     each(z_copy, z, NZ, receive)
-    total = jnp.sum(redz[...], axis=0)
+    both = jnp.zeros((1, 1024), F32)
+    for block in range(NZ):
+        both = both + block_factor[8 * block : 8 * block + 1] * redz[block]
+    total = both[:, :512] + both[:, 512:]
     for h in range(8):
-        tot8[h : h + 1, :] = total[h // 2 : h // 2 + 1, (h % 2) * 64 : (h % 2) * 64 + 64]
-    gated = tot8[...] * jax.nn.silu(gateb[0].astype(F32))
+        tot8[h : h + 1, :] = total[:, h * P_SIZE : (h + 1) * P_SIZE]
+    gated = tot8[...] * gate
     squares = jnp.sum(jnp.sum(gated * gated, axis=0, keepdims=True), axis=1, keepdims=True)
     reds[tp] = jnp.broadcast_to(squares, (1, 128))
     each(s_copy, tp, NTP, start)
     each(s_copy, tp, NTP, receive)
     square_sum = jnp.sum(reds[...], axis=0)[:, :64]
     scale = lax.rsqrt(square_sum / (H * P_SIZE) + EPSILON)
-    tot8[...] = gated * scale * gainb[...]
-    gateb[0] = tot8[...].astype(BF16)
-    final = pltpu.make_async_copy(gateb, first_read, fsem)
-    final.start()
-
-    def state_arrives(i, carry):
-        s = (sp + i) % NSP
-        state_copy(s, s).wait_recv()
-        return carry
+    first_read[0] = (gated * scale * gainb[...]).astype(BF16)
 
     for c in sent:
         c.wait_send()
     edge_up().wait_send()
     edge_down().wait_send()
-    each(closing_copy, sp, NSP, leave)
+    each(closing_copy, y, NY, leave)
+    each(block_copy, z, NZ, leave)
     each(y_copy, y, NY, leave)
     each(z_copy, z, NZ, leave)
     each(s_copy, tp, NTP, leave)
-    lax.fori_loop(1, NSP, state_arrives, 0)
-    each(state_copy, sp, NSP, leave)
-    own_out.wait()
-    final.wait()
+    for k in range(2):
+        each(functools.partial(state_copy, k), sp, NSP, receive)
+        each(functools.partial(state_copy, k), sp, NSP, leave)
+        own_out[k].wait()
 
 
 def per_device(*args):
     dma = pltpu.SemaphoreType.DMA
     any_spec = pl.BlockSpec(memory_space=pl.ANY)
+    vmem_spec = pl.BlockSpec(memory_space=pltpu.VMEM)
+    shapes = (
+        jax.ShapeDtypeStruct((64, 2, 8, 256), BF16),
+        jax.ShapeDtypeStruct((1, 8, 64), BF16),
+    )
     return pl.pallas_call(
         kernel,
-        out_shape=(
-            jax.ShapeDtypeStruct((64, 2, 8, 256), BF16),
-            jax.ShapeDtypeStruct((1, 8, 64), BF16),
-        ),
+        out_shape=tuple(pltpu.VMEM(t.shape, t.dtype) for t in shapes),
         in_specs=[any_spec] * 12,
-        out_specs=(any_spec, any_spec),
+        out_specs=(vmem_spec, vmem_spec),
         scratch_shapes=[
             pltpu.VMEM((NTP, TOK, FEAT), BF16),
             pltpu.VMEM((2048, WC), BF16),
@@ -487,13 +528,14 @@
             pltpu.VMEM((1, 8, P_SIZE), BF16),
             pltpu.VMEM((8, P_SIZE), F32),
             pltpu.SMEM((1,), jnp.int32),
-            pltpu.VMEM((NSP, 2, 128), F32),
+            pltpu.VMEM((NY, 2, 128), F32),
+            pltpu.VMEM((NZ, 1, 128), F32),
             pltpu.VMEM((256, 1024), BF16),
             pltpu.VMEM((2, 256, 128), F32),
             pltpu.VMEM((NSP, 2, 2, 8, 256), BF16),
-            pltpu.VMEM((8, 512), F32),
-            pltpu.VMEM((NY, 4, 128), F32),
-            pltpu.VMEM((NZ, 4, 128), F32),
+            pltpu.VMEM((8, 1024), F32),
+            pltpu.VMEM((NY, 1, 1024), F32),
+            pltpu.VMEM((NZ, 1, 1024), F32),
             pltpu.VMEM((NTP, 1, 128), F32),
             pltpu.VMEM((8, P_SIZE), F32),
             dma,
@@ -502,18 +544,20 @@
             dma((NTP, CH)),
             dma((2,)),
             dma((2,)),
-            dma((NSP,)),
-            dma((NSP,)),
-            dma((NSP,)),
-            dma((NSP,)),
+            dma((NY,)),
+            dma((NY,)),
+            dma((2, NSP)),
+            dma((2, NSP)),
             dma((NY,)),
             dma((NY,)),
             dma((NZ,)),
             dma((NZ,)),
+            dma((NZ,)),
+            dma((NZ,)),
             dma((NTP,)),
             dma((NTP,)),
-            dma,
-            dma,
+            dma((2,)),
+            pltpu.SemaphoreType.REGULAR((3,)),
         ],
         compiler_params=pltpu.CompilerParams(collective_id=0, has_side_effects=True),
     )(*args)

time: 56 us -> 47.9 us (0.86)
  Pallas kernels: 50.9 us -> 45.1 us
  local copies, waits for them, and re-layouts: 3.12 us -> 1.37 us
    pallas_call x1, Pallas kernels: 50.9 us -> 45.1 us  [per_device(): pl.pallas_call(kernel, out_shape=tuple((pltpu.VMEM(t.shape, t.dtype) for...]
    unnamed x2, local copies, waits for them, and re-layouts: 3.12 us -> 1.37 us
where the time goes in v2:
time: 47.9 us; the launch traced here: 47.7 us
  Pallas kernels  45.1 us (94%)
  local copies, waits for them, and re-layouts  1.37 us (3%)
  between operations  1.29 us (3%)
    pallas_call x1, Pallas kernels, per_device(): pl.pallas_call(kernel, out_shape=tuple((pltpu.VMEM(t.shape, t.dtype) for...  45.1 us
    unnamed x2, local copies, waits for them, and re-layouts  1.37 us

profile of v2, /device:TPU:1, one launch (start us, length us, event | category | flops | bytes accessed | tf_op | source)
XLA Modules:
  0.0 47.7 jit_solution(665346340893910301)
XLA Ops:
  1.3 45.1 %shard_map.131 = (bf16[64,2,8,256]{3,2,1,0:T(8,128)(2,1)S(1)}, bf16[1,8,64]{2,1,0:T(8,128)(2,1)S(1)}) custom-call(bf16[256,256]{1,0:T(8,128)(2,1)} %inputs.1, bf16[2048,512]{1,0:T(8,128)(2,1)} %x_weight.1, bf16[2048,256]{1,0:T(8,128)(2,1)} %b_weight.1, bf16[2048,128]{1,0:T(8,128)(2,1)} %dt_weight.1, f32[2,64]{1,0:T(2,128)} %dt_bias.1, f32[2,64]{1,0:T(2,128)} %decay_rate.1, ...), custom_call_target="tpu_custom_call" | custom-call | tf_op jit(solution)/shard_map/pallas_call | solution.py:512
  46.4 0.8 %copy.16 = bf16[64,2,8,256]{3,2,1,0:T(8,128)(2,1)} copy(bf16[64,2,8,256]{3,2,1,0:T(8,128)(2,1)S(1)} %get-tuple-element.2) | data formatting | bytes 1048576
  47.2 0.6 %copy.17 = bf16[1,8,64]{2,1,0:T(8,128)(2,1)} copy(bf16[1,8,64]{2,1,0:T(8,128)(2,1)S(1)} %get-tuple-element.3) | data formatting | bytes 2048

commit v3 on v2

v3 whole, which is shorter than its diff:
```python
import functools
import jax
import jax.numpy as jnp
from jax import lax
from jax.experimental import pallas as pl
from jax.experimental.pallas import tpu as pltpu
from jax.sharding import PartitionSpec as P

H = 64
P_SIZE = 64
G = 16
N = 128
KW = 5
SPAN = 128
EPSILON = 1e-06
LEN = 8192
NY = 8
NZ = 4
NX = 4
NSP = 32
NTP = 8
TOK = 256
FEAT = 256
XC = 512
BC = 256
CC = 768
WC = 896
EDGE = 16
ROWS_A = 144
ROWS_B = TOK - ROWS_A
TOP = EDGE + ROWS_A
EARLY = 3

MESH = pl.DeviceIdType.MESH
F32 = jnp.float32
BF16 = jnp.bfloat16


def iota(shape, dim):
    return lax.broadcasted_iota(jnp.int32, shape, dim)


def kernel(
    inputs, x_weight, b_weight, dt_weight, dt_bias, decay_rate, conv_x, conv_b,
    query_c, query_gate, read_span, read_gain,
    cache, first_read,
    slab, wbuf, acc, proj, mixed, biasb, rateb, cxb, cbb, qb, gateb, gainb, rb,
    expand, sbuf, sendb, ybuf, redy, redz, reds, tot8,
    in_sem, load_sems, gsend, grecv, hsend, hrecv, asend, arecv,
    ysend, yrecv, zsend, zrecv, ssend, srecv, own_sem, stage,
):
    sp = lax.axis_index("sp")
    tp = lax.axis_index("tp")
    y = sp % NY
    z = sp // NY
    x = tp // 2
    core = tp % 2
    partner = 2 * x + 1 - core
    right = 2 * ((x + 1) % NX) + core
    left = 2 * ((x + NX - 1) % NX) + core
    across = 2 * ((x + 2) % NX) + core

    own_in = pltpu.make_async_copy(inputs, slab.at[tp, pl.ds(EDGE, TOK), :], in_sem)
    own_in.start()
    loads = [
        (x_weight, wbuf.at[:, pl.ds(0, XC)]),
        (b_weight, wbuf.at[:, pl.ds(XC, BC)]),
        (dt_weight, wbuf.at[:, pl.ds(CC, 128)]),
        (dt_bias, biasb),
        (decay_rate, rateb),
        (conv_x, cxb),
        (conv_b, cbb),
        (query_c, qb),
        (query_gate, gateb),
        (read_gain, gainb),
        (read_span, rb),
    ]
    copies = []
    for i, (src, dst) in enumerate(loads):
        c = pltpu.make_async_copy(src, dst, load_sems.at[i])
        c.start()
        copies.append(c)

    barrier = pltpu.get_barrier_semaphore()

    def at_y(other):
        return {"sp": z * NY + (other + NY) % NY}

    def greet_tp(i, carry):
        pl.semaphore_signal(
            barrier, inc=1, device_id={"tp": (tp + i) % NTP}, device_id_type=MESH
        )
        return carry

    def greet_z(i, carry):
        pl.semaphore_signal(
            barrier, inc=1, device_id={"sp": ((z + i) % NZ) * NY + y}, device_id_type=MESH
        )
        return carry

    lax.fori_loop(1, NTP, greet_tp, 0)
    lax.fori_loop(1, NZ, greet_z, 0)
    for side in (1, -1):
        pl.semaphore_signal(barrier, inc=1, device_id=at_y(y + side), device_id_type=MESH)
        pl.semaphore_signal(
            barrier, inc=1, device_id={"sp": (sp + NSP + side) % NSP}, device_id_type=MESH
        )

    def tell(index, distance):
        for side in (distance, -distance):
            pl.semaphore_signal(
                stage.at[index], inc=1, device_id=at_y(y + side), device_id_type=MESH
            )

    er = iota((256, 1024), 0) % 128
    ec = iota((256, 1024), 1)
    expand[...] = jnp.where(
        er == (ec // 512) * H + tp * 8 + (ec % 512) // P_SIZE, 1.0, 0.0
    ).astype(BF16)

    @pl.when(sp == 0)
    def _():
        slab[tp, pl.ds(0, EDGE), :] = jnp.zeros((EDGE, FEAT), BF16)

    own_in.wait()
    pl.semaphore_wait(barrier, NTP - 1 + NZ - 1 + 4)
    tell(0, 1)

    def edge_in():
        return pltpu.make_async_remote_copy(
            src_ref=slab.at[tp, pl.ds(TOK, EDGE), :],
            dst_ref=slab.at[tp, pl.ds(0, EDGE), :],
            send_sem=hsend.at[0],
            recv_sem=hrecv.at[0],
            device_id={"sp": (sp + 1) % NSP},
            device_id_type=MESH,
        )

    @pl.when(sp < NSP - 1)
    def _():
        edge_in().start()

    pieces = [(EDGE, ROWS_A), (0, EDGE), (TOP, ROWS_B)]
    sent = []

    def part(slot, j):
        return slab.at[slot, pl.ds(*pieces[j]), :]

    def forward(slot, j, dest, index):
        c = pltpu.make_async_remote_copy(
            src_ref=part(slot, j),
            dst_ref=part(slot, j),
            send_sem=gsend.at[index, j],
            recv_sem=grecv.at[slot, j],
            device_id={"tp": dest},
            device_id_type=MESH,
        )
        c.start()
        sent.append(c)

    def arrive(slot, j):
        pltpu.make_async_remote_copy(
            src_ref=part(slot, j),
            dst_ref=part(slot, j),
            send_sem=gsend.at[0, j],
            recv_sem=grecv.at[slot, j],
            device_id={"tp": partner},
            device_id_type=MESH,
        ).wait_recv()

    def send_own(j):
        for index, dest in enumerate((across, right, left, partner)):
            forward(tp, j, dest, index)

    ring = (right, left, across)

    def pass_on(j):
        for index, slot in enumerate(ring):
            arrive(slot, j)
            forward(slot, j, partner, 4 + index)

    def twin(slot):
        return slot + 1 - 2 * core

    def product(slot, start, count):
        rows = pl.ds(pl.multiple_of(slot * FEAT, FEAT), FEAT)
        return jnp.dot(
            slab[slot, pl.ds(start, count), :], wbuf[rows, :], preferred_element_type=F32
        )

    def add(slot, start, count):
        acc[pl.ds(start, count), :] += product(slot, start, count)

    send_own(0)
    for c in copies:
        c.wait()
    acc[pl.ds(TOP, ROWS_B), :] = product(tp, TOP, ROWS_B)

    @pl.when(sp > 0)
    def _():
        edge_in().wait_recv()

    send_own(1)
    send_own(2)
    acc[pl.ds(0, TOP), :] = product(tp, 0, TOP)
    for j in (0, 1):
        arrive(partner, j)
    add(partner, 0, TOP)
    pass_on(0)
    pl.semaphore_wait(stage.at[0], 2)
    tell(1, 2)
    pass_on(1)
    for slot in ring:
        add(slot, 0, TOP)
    for slot in ring[:2]:
        for j in (0, 1):
            arrive(twin(slot), j)
        add(twin(slot), 0, TOP)
    pl.semaphore_wait(stage.at[1], 2)
    tell(2, 1)
    for j in (0, 1):
        arrive(twin(across), j)
    last = product(twin(across), 0, TOP)
    proj[pl.ds(0, TOP), :] = (acc[pl.ds(0, TOP), :CC] + last[:, :CC]).astype(BF16).astype(F32)
    acc[pl.ds(0, TOP), CC:] += last[:, CC:]

    @pl.when(sp == 0)
    def _():
        proj[pl.ds(0, EDGE), :] = jnp.zeros((EDGE, CC), F32)

    def edge_down():
        return pltpu.make_async_remote_copy(
            src_ref=proj.at[pl.ds(EDGE, 8), :],
            dst_ref=proj.at[pl.ds(EDGE + TOK, 8), :],
            send_sem=hsend.at[1],
            recv_sem=hrecv.at[1],
            device_id={"sp": (sp + NSP - 1) % NSP},
            device_id_type=MESH,
        )

    @pl.when(sp > 0)
    def _():
        edge_down().start()

    bias = jnp.concatenate([biasb[0:1, :], biasb[1:2, :]], axis=1)
    rate = jnp.concatenate([rateb[0:1, :], rateb[1:2, :]], axis=1)
    row = iota((SPAN, SPAN), 0)
    col = iota((SPAN, SPAN), 1)
    later = jnp.where(col > row, 1.0, 0.0)
    earlier = jnp.where(col < row, 1.0, 0.0)

    def weights_of(k):
        dt_raw = acc[pl.ds(EDGE + k * SPAN, SPAN), CC:].astype(BF16).astype(F32)
        v = dt_raw + bias
        step = jnp.maximum(v, 0.0) + jnp.log1p(jnp.exp(-jnp.abs(v)))
        a = -(step * rate) / LEN
        tail = jnp.dot(later, a, precision=lax.Precision.HIGHEST, preferred_element_type=F32)
        head = jnp.dot(earlier, a, precision=lax.Precision.HIGHEST, preferred_element_type=F32)
        w = jnp.exp(jnp.where(col < H, tail, head)) * step
        redy[y, k : k + 1, pl.ds(512, 128)] = jnp.sum(a, axis=0, keepdims=True)
        high = w.astype(BF16)
        low = (w - high.astype(F32)).astype(BF16)
        return jnp.concatenate([high, low], axis=1)

    taps = [cxb[...].astype(F32), cbb[...].astype(F32)]

    def convolve(start, count):
        for block in range(CC // 256):
            tap = taps[0][:, block * 256 : (block + 1) * 256] if block < 2 else taps[1]
            cols = pl.ds(block * 256, 256)
            total = jnp.zeros((count, 256), F32)
            for o in range(KW):
                total = total + tap[o : o + 1] * proj[pl.ds(start + EDGE - 2 + o, count), cols]
            mixed[pl.ds(start, count), cols] = jax.nn.silu(total).astype(BF16)

    order = (4 * (row % 32) + row // 32 == col)
    order_t = jnp.where(order, 1.0, 0.0).astype(BF16)
    contract_last = (((1,), (1,)), ((), ()))
    queries = []
    for g in range(2):
        q8 = jnp.broadcast_to(qb[0, g : g + 1, :].astype(F32), (8, N)).astype(BF16)
        queries.append(
            lax.dot_general(q8, order_t, contract_last, preferred_element_type=F32).astype(BF16)
        )
    half = iota((32, 128), 1) < P_SIZE
    chosen = rb[0]

    def state_copy(k, d, s):
        return pltpu.make_async_remote_copy(
            src_ref=sendb.at[d, k],
            dst_ref=cache.at[2 * s + k],
            send_sem=asend.at[k, d],
            recv_sem=arecv.at[k, s],
            device_id={"sp": d},
            device_id_type=MESH,
        )

    def send_states(k, first, last):
        def body(i, carry):
            m = 7 - (first + i // NZ)
            dy = (m % 2) * ((m + 1) // 2) + (1 - m % 2) * (8 - m // 2)
            d = ((z + i % NZ) % NZ) * NY + (y + dy) % NY
            state_copy(k, d, sp).start()
            return carry

        lax.fori_loop(0, (last - first) * NZ, body, 0)

    def send_column(k):
        def body(i, carry):
            state_copy(k, ((z + i) % NZ) * NY + y, sp).start()
            return carry

        lax.fori_loop(1, NZ, body, 0)

    own_out = []

    def states_of(k, pair):
        rows = pl.ds(k * SPAN, SPAN)
        keys_t = [
            lax.dot_general(
                order_t, mixed[rows, pl.ds(XC + g * N, N)], contract_last,
                preferred_element_type=F32,
            ).astype(BF16)
            for g in range(2)
        ]
        for e in range(2):
            wide = jnp.dot(pair, expand[:, pl.ds(e * 512, 512)], preferred_element_type=F32)
            weighted = (mixed[rows, pl.ds(0, XC)].astype(F32) * wide).astype(BF16)
            for g in range(2):
                state = jnp.dot(
                    keys_t[g], weighted[:, g * 256 : (g + 1) * 256], preferred_element_type=F32
                )
                read = jnp.dot(queries[g], state.astype(BF16), preferred_element_type=F32)
                ybuf[e : e + 1, pl.ds(g * 256, 256)] = read[0:1]
                for j in range(2):
                    for a in range(2):
                        one = state[64 * a : 64 * a + 32, 128 * j : 128 * j + 128]
                        two = state[64 * a + 32 : 64 * a + 64, 128 * j : 128 * j + 128]
                        first = jnp.where(half, one, pltpu.roll(two, 64, 1))
                        second = jnp.where(half, pltpu.roll(one, 64, 1), two)
                        h = 4 * g + 2 * j
                        sbuf[a, pl.ds(h, 32, stride=8), :] = first
                        sbuf[a, pl.ds(h + 1, 32, stride=8), :] = second
            for a in range(2):
                sendb[:, k, e, :, pl.ds(a * 128, 128)] = (
                    sbuf[a].reshape(NSP, 8, 128).astype(BF16)
                )
        at = jnp.full((1, 512), 2 * sp + k, jnp.int32)
        pick = jnp.full((1, 512), chosen, jnp.int32)
        redy[y, k : k + 1, pl.ds(0, 512)] = jnp.where(at <= pick, ybuf[0:1, :], 0.0) + jnp.where(
            at >= pick, ybuf[1:2, :], 0.0
        )
        c = pltpu.make_async_copy(sendb.at[sp, k], cache.at[2 * sp + k], own_sem.at[k])
        c.start()
        own_out.append(c)

    pair = weights_of(0)
    for first in range(0, SPAN, 16):
        convolve(first, 16)
    pass_on(2)
    pl.semaphore_wait(stage.at[2], 2)
    states_of(0, pair)
    send_column(0)
    send_states(0, 0, EARLY)

    for slot in (partner, *ring, twin(right), twin(left)):
        if slot is not right and slot is not left and slot is not across:
            arrive(slot, 2)
        add(slot, TOP, ROWS_B)
    arrive(twin(across), 2)
    last = product(twin(across), TOP, ROWS_B)
    rest = pl.ds(TOP, ROWS_B)
    proj[rest, :] = (acc[rest, :CC] + last[:, :CC]).astype(BF16).astype(F32)
    acc[rest, CC:] += last[:, CC:]
    pair = weights_of(1)
    for first in range(SPAN, TOK - 16, 16):
        convolve(first, 16)

    @pl.when(sp < NSP - 1)
    def _():
        edge_down().wait_recv()

    @pl.when(sp == NSP - 1)
    def _():
        proj[pl.ds(EDGE + TOK, 8), :] = jnp.zeros((8, CC), F32)

    convolve(TOK - 16, 16)
    states_of(1, pair)

    def y_copy(d, s):
        return pltpu.make_async_remote_copy(
            src_ref=redy.at[s],
            dst_ref=redy.at[s],
            send_sem=ysend.at[d],
            recv_sem=yrecv.at[s],
            device_id=at_y(d),
            device_id_type=MESH,
        )

    def z_copy(d, s):
        return pltpu.make_async_remote_copy(
            src_ref=redz.at[s],
            dst_ref=redz.at[s],
            send_sem=zsend.at[d],
            recv_sem=zrecv.at[s],
            device_id={"sp": d * NY + y},
            device_id_type=MESH,
        )

    def s_copy(d, s):
        return pltpu.make_async_remote_copy(
            src_ref=reds.at[s],
            dst_ref=reds.at[s],
            send_sem=ssend.at[d],
            recv_sem=srecv.at[s],
            device_id={"tp": d},
            device_id_type=MESH,
        )

    def each(copy, me, count, act):
        def body(i, carry):
            act(copy, me, (me + i) % count)
            return carry

        lax.fori_loop(1, count, body, 0)

    def start(copy, me, other):
        copy(other, me).start()

    def receive(copy, me, other):
        copy(other, other).wait_recv()

    def leave(copy, me, other):
        copy(other, me).wait_send()

    each(y_copy, y, NY, start)
    send_states(0, EARLY, 7)
    send_column(1)
    send_states(1, 0, 7)

    def spread(rows):
        high = rows.astype(BF16)
        low = (rows - high.astype(F32)).astype(BF16)
        return jnp.dot(
            jnp.concatenate([high, low], axis=1),
            expand[:, pl.ds(0, 512)],
            preferred_element_type=F32,
        )

    gate = jax.nn.silu(gateb[0].astype(F32))
    each(y_copy, y, NY, receive)
    base = 2 * NY * z
    ahead_lane = iota((8, 128), 1) < H
    block_log = jnp.zeros((8, 128), F32)
    span_logs = [jnp.zeros((8, 128), F32), jnp.zeros((8, 128), F32)]
    pick = jnp.full((8, 128), chosen, jnp.int32)
    span_at = [base + 2 * iota((8, 128), 0) + k for k in range(2)]
    for other in range(2 * NY):
        log = jnp.broadcast_to(
            redy[other // 2, other % 2 : other % 2 + 1, pl.ds(512, 128)], (8, 128)
        )
        here = jnp.full((8, 128), base + other, jnp.int32)
        log = jnp.where(ahead_lane, jnp.where(here <= pick, log, 0.0), jnp.where(here >= pick, log, 0.0))
        block_log = block_log + log
        for k in range(2):
            counted = jnp.where(
                ahead_lane,
                jnp.where(here > span_at[k], log, 0.0),
                jnp.where(here < span_at[k], log, 0.0),
            )
            span_logs[k] = span_logs[k] + counted
    span_weights = [jnp.exp(t + pltpu.roll(t, H, 1)) for t in span_logs]
    wide_weight = spread(jnp.concatenate(span_weights, axis=0))
    partial = jnp.zeros((8, 512), F32)
    for k in range(2):
        partial = partial + wide_weight[8 * k : 8 * k + 8] * redy[:, k, pl.ds(0, 512)]
    redz[z, :, pl.ds(0, 512)] = jnp.sum(partial, axis=0, keepdims=True)
    redz[z, :, pl.ds(512, 128)] = block_log[0:1]
    each(z_copy, z, NZ, start)
    each(z_copy, z, NZ, receive)
    lane = iota((1, 128), 1)
    block_rows = []
    for block in range(NZ):
        after = jnp.zeros((1, 128), F32)
        before = jnp.zeros((1, 128), F32)
        for other in range(block + 1, NZ):
            after = after + redz[other, :, pl.ds(512, 128)]
        for other in range(block):
            before = before + redz[other, :, pl.ds(512, 128)]
        block_rows.append(jnp.where(lane < H, after, before))
    block_rows = block_rows + [jnp.zeros((8 - NZ, 128), F32)]
    logs = jnp.concatenate(block_rows, axis=0)
    block_factor = spread(jnp.exp(logs + pltpu.roll(logs, H, 1)))
    total = jnp.zeros((1, 512), F32)
    for block in range(NZ):
        total = total + block_factor[block : block + 1] * redz[block, :, pl.ds(0, 512)]
    for h in range(8):
        tot8[h : h + 1, :] = total[:, h * P_SIZE : (h + 1) * P_SIZE]
    gated = tot8[...] * gate
    squares = jnp.sum(jnp.sum(gated * gated, axis=0, keepdims=True), axis=1, keepdims=True)
    reds[tp] = jnp.broadcast_to(squares, (1, 128))
    each(s_copy, tp, NTP, start)
    each(s_copy, tp, NTP, receive)
    square_sum = jnp.sum(reds[...], axis=0)[:, :64]
    scale = lax.rsqrt(square_sum / (H * P_SIZE) + EPSILON)
    first_read[0] = (gated * scale * gainb[...]).astype(BF16)

    for c in sent:
        c.wait_send()

    @pl.when(sp < NSP - 1)
    def _():
        edge_in().wait_send()

    @pl.when(sp > 0)
    def _():
        edge_down().wait_send()

    each(y_copy, y, NY, leave)
    each(z_copy, z, NZ, leave)
    each(s_copy, tp, NTP, leave)
    for k in range(2):
        each(functools.partial(state_copy, k), sp, NSP, receive)
        each(functools.partial(state_copy, k), sp, NSP, leave)
        own_out[k].wait()


def per_device(*args):
    dma = pltpu.SemaphoreType.DMA
    any_spec = pl.BlockSpec(memory_space=pl.ANY)
    vmem_spec = pl.BlockSpec(memory_space=pltpu.VMEM)
    shapes = (
        jax.ShapeDtypeStruct((64, 2, 8, 256), BF16),
        jax.ShapeDtypeStruct((1, 8, 64), BF16),
    )
    return pl.pallas_call(
        kernel,
        out_shape=tuple(pltpu.VMEM(t.shape, t.dtype) for t in shapes),
        in_specs=[any_spec] * 12,
        out_specs=(vmem_spec, vmem_spec),
        scratch_shapes=[
            pltpu.VMEM((NTP, EDGE + TOK, FEAT), BF16),
            pltpu.VMEM((2048, WC), BF16),
            pltpu.VMEM((EDGE + TOK, WC), F32),
            pltpu.VMEM((EDGE + TOK + 8, CC), F32),
            pltpu.VMEM((TOK, CC), BF16),
            pltpu.VMEM((2, H), F32),
            pltpu.VMEM((2, H), F32),
            pltpu.VMEM((KW, XC), BF16),
            pltpu.VMEM((KW, BC), BF16),
            pltpu.VMEM((1, 2, N), BF16),
            pltpu.VMEM((1, 8, P_SIZE), BF16),
            pltpu.VMEM((8, P_SIZE), F32),
            pltpu.SMEM((1,), jnp.int32),
            pltpu.VMEM((256, 1024), BF16),
            pltpu.VMEM((2, 256, 128), F32),
            pltpu.VMEM((NSP, 2, 2, 8, 256), BF16),
            pltpu.VMEM((8, 512), F32),
            pltpu.VMEM((NY, 2, 640), F32),
            pltpu.VMEM((NZ, 1, 640), F32),
            pltpu.VMEM((NTP, 1, 128), F32),
            pltpu.VMEM((8, P_SIZE), F32),
            dma,
            dma((11,)),
            dma((7, 3)),
            dma((NTP, 3)),
            dma((2,)),
            dma((2,)),
            dma((2, NSP)),
            dma((2, NSP)),
            dma((NY,)),
            dma((NY,)),
            dma((NZ,)),
            dma((NZ,)),
            dma((NTP,)),
            dma((NTP,)),
            dma((2,)),
            pltpu.SemaphoreType.REGULAR((3,)),
        ],
        compiler_params=pltpu.CompilerParams(collective_id=0, has_side_effects=True),
    )(*args)


def solution(mesh):
    return jax.shard_map(
        per_device,
        mesh=mesh,
        in_specs=(
            P(("gr", "sp"), "tp"),
            P(None, "tp"),
            P(None, "tp"),
            P(),
            P(),
            P(),
            P(None, "tp"),
            P(None, "tp"),
            P("gr", "tp", None),
            P("gr", "tp", None),
            P("gr"),
            P("tp", None),
        ),
        out_specs=(P("gr", None, "tp", "sp"), P("gr", "tp", None)),
        check_vma=False,
    )
```

time: 47.9 us -> 45.4 us (0.948)
  Pallas kernels: 45.1 us -> 42.6 us
    pallas_call x1, Pallas kernels: 45.1 us -> 42.6 us  [per_device(): pl.pallas_call(kernel, out_shape=tuple((pltpu.VMEM(t.shape, t.dtype) for...]
where the time goes in v3:
time: 45.4 us; the launch traced here: 45.3 us
  Pallas kernels  42.6 us (94%)
  local copies, waits for them, and re-layouts  1.37 us (3%)
  between operations  1.29 us (3%)
    pallas_call x1, Pallas kernels, per_device(): pl.pallas_call(kernel, out_shape=tuple((pltpu.VMEM(t.shape, t.dtype) for...  42.6 us
    unnamed x2, local copies, waits for them, and re-layouts  1.37 us

profile of v3, /device:TPU:1, one launch (start us, length us, event | category | flops | bytes accessed | tf_op | source)
XLA Modules:
  0.0 45.3 jit_solution(12523373888016924522)
XLA Ops:
  1.3 42.6 %shard_map.131 = (bf16[64,2,8,256]{3,2,1,0:T(8,128)(2,1)S(1)}, bf16[1,8,64]{2,1,0:T(8,128)(2,1)S(1)}) custom-call(bf16[256,256]{1,0:T(8,128)(2,1)} %inputs.1, bf16[2048,512]{1,0:T(8,128)(2,1)} %x_weight.1, bf16[2048,256]{1,0:T(8,128)(2,1)} %b_weight.1, bf16[2048,128]{1,0:T(8,128)(2,1)} %dt_weight.1, f32[2,64]{1,0:T(2,128)} %dt_bias.1, f32[2,64]{1,0:T(2,128)} %decay_rate.1, ...), custom_call_target="tpu_custom_call" | custom-call | tf_op jit(solution)/shard_map/pallas_call | solution.py:536
  43.9 0.8 %copy.16 = bf16[64,2,8,256]{3,2,1,0:T(8,128)(2,1)} copy(bf16[64,2,8,256]{3,2,1,0:T(8,128)(2,1)S(1)} %get-tuple-element.2) | data formatting | bytes 1048576
  44.7 0.6 %copy.17 = bf16[1,8,64]{2,1,0:T(8,128)(2,1)} copy(bf16[1,8,64]{2,1,0:T(8,128)(2,1)S(1)} %get-tuple-element.3) | data formatting | bytes 2048

commit v4 on v3

--- a/solution.py
+++ b/solution.py
@@ -1,4 +1,3 @@
-import functools
 import jax
 import jax.numpy as jnp
 from jax import lax
@@ -30,6 +29,7 @@
 ROWS_B = TOK - ROWS_A
 TOP = EDGE + ROWS_A
 EARLY = 3
+MID = 0
 
 MESH = pl.DeviceIdType.MESH
 F32 = jnp.float32
@@ -44,10 +44,10 @@
     inputs, x_weight, b_weight, dt_weight, dt_bias, decay_rate, conv_x, conv_b,
     query_c, query_gate, read_span, read_gain,
     cache, first_read,
-    slab, wbuf, acc, proj, mixed, biasb, rateb, cxb, cbb, qb, gateb, gainb, rb,
+    slab, wbuf, acc, proj, mixed, held, biasb, rateb, cxb, cbb, qb, gateb, gainb, rb,
     expand, sbuf, sendb, ybuf, redy, redz, reds, tot8,
     in_sem, load_sems, gsend, grecv, hsend, hrecv, asend, arecv,
-    ysend, yrecv, zsend, zrecv, ssend, srecv, own_sem, stage,
+    ysems, zsems, ssems, own_sem, stage,
 ):
     sp = lax.axis_index("sp")
     tp = lax.axis_index("tp")
@@ -112,12 +112,6 @@
                 stage.at[index], inc=1, device_id=at_y(y + side), device_id_type=MESH
             )
 
-    er = iota((256, 1024), 0) % 128
-    ec = iota((256, 1024), 1)
-    expand[...] = jnp.where(
-        er == (ec // 512) * H + tp * 8 + (ec % 512) // P_SIZE, 1.0, 0.0
-    ).astype(BF16)
-
     @pl.when(sp == 0)
     def _():
         slab[tp, pl.ds(0, EDGE), :] = jnp.zeros((EDGE, FEAT), BF16)
@@ -141,43 +135,41 @@
         edge_in().start()
 
     pieces = [(EDGE, ROWS_A), (0, EDGE), (TOP, ROWS_B)]
-    sent = []
 
     def part(slot, j):
         return slab.at[slot, pl.ds(*pieces[j]), :]
 
-    def forward(slot, j, dest, index):
+    def forward(slot, j, dest):
         c = pltpu.make_async_remote_copy(
             src_ref=part(slot, j),
             dst_ref=part(slot, j),
-            send_sem=gsend.at[index, j],
+            send_sem=gsend.at[j],
             recv_sem=grecv.at[slot, j],
             device_id={"tp": dest},
             device_id_type=MESH,
         )
         c.start()
-        sent.append(c)
 
     def arrive(slot, j):
         pltpu.make_async_remote_copy(
             src_ref=part(slot, j),
             dst_ref=part(slot, j),
-            send_sem=gsend.at[0, j],
+            send_sem=gsend.at[j],
             recv_sem=grecv.at[slot, j],
             device_id={"tp": partner},
             device_id_type=MESH,
         ).wait_recv()
 
     def send_own(j):
-        for index, dest in enumerate((across, right, left, partner)):
-            forward(tp, j, dest, index)
+        for dest in (across, right, left, partner):
+            forward(tp, j, dest)
 
     ring = (right, left, across)
 
     def pass_on(j):
-        for index, slot in enumerate(ring):
+        for slot in ring:
             arrive(slot, j)
-            forward(slot, j, partner, 4 + index)
+            forward(slot, j, partner)
 
     def twin(slot):
         return slot + 1 - 2 * core
@@ -192,16 +184,21 @@
         acc[pl.ds(start, count), :] += product(slot, start, count)
 
     send_own(0)
+    er = iota((256, 1024), 0) % 128
+    ec = iota((256, 1024), 1)
+    expand[...] = jnp.where(
+        er == (ec // 512) * H + tp * 8 + (ec % 512) // P_SIZE, 1.0, 0.0
+    ).astype(BF16)
+
+    @pl.when(sp > 0)
+    def _():
+        edge_in().wait_recv()
+
+    send_own(1)
+    send_own(2)
     for c in copies:
         c.wait()
     acc[pl.ds(TOP, ROWS_B), :] = product(tp, TOP, ROWS_B)
-
-    @pl.when(sp > 0)
-    def _():
-        edge_in().wait_recv()
-
-    send_own(1)
-    send_own(2)
     acc[pl.ds(0, TOP), :] = product(tp, 0, TOP)
     for j in (0, 1):
         arrive(partner, j)
@@ -289,28 +286,24 @@
         return pltpu.make_async_remote_copy(
             src_ref=sendb.at[d, k],
             dst_ref=cache.at[2 * s + k],
-            send_sem=asend.at[k, d],
-            recv_sem=arecv.at[k, s],
+            send_sem=asend,
+            recv_sem=arecv,
             device_id={"sp": d},
             device_id_type=MESH,
         )
 
+    across_y = [lax.rem(y + dy, NY) for dy in range(NY)]
+    across_z = [lax.rem(z + dz, NZ) * NY for dz in range(NZ)]
+    distances = (4, 5, 3, 6, 2, 7, 1)
+
     def send_states(k, first, last):
-        def body(i, carry):
-            m = 7 - (first + i // NZ)
-            dy = (m % 2) * ((m + 1) // 2) + (1 - m % 2) * (8 - m // 2)
-            d = ((z + i % NZ) % NZ) * NY + (y + dy) % NY
-            state_copy(k, d, sp).start()
-            return carry
-
-        lax.fori_loop(0, (last - first) * NZ, body, 0)
+        for dy in distances[first:last]:
+            for dz in range(NZ):
+                state_copy(k, across_z[dz] + across_y[dy], sp).start()
 
     def send_column(k):
-        def body(i, carry):
-            state_copy(k, ((z + i) % NZ) * NY + y, sp).start()
-            return carry
-
-        lax.fori_loop(1, NZ, body, 0)
+        for dz in range(1, NZ):
+            state_copy(k, across_z[dz] + y, sp).start()
 
     own_out = []
 
@@ -332,10 +325,21 @@
                 )
                 read = jnp.dot(queries[g], state.astype(BF16), preferred_element_type=F32)
                 ybuf[e : e + 1, pl.ds(g * 256, 256)] = read[0:1]
+                held[e, g] = state
+        at = jnp.full((1, 512), 2 * sp + k, jnp.int32)
+        pick = jnp.full((1, 512), chosen, jnp.int32)
+        redy[y, k : k + 1, pl.ds(0, 512)] = jnp.where(at <= pick, ybuf[0:1, :], 0.0) + jnp.where(
+            at >= pick, ybuf[1:2, :], 0.0
+        )
+
+    def arrange(k):
+        for e in range(2):
+            for g in range(2):
                 for j in range(2):
                     for a in range(2):
-                        one = state[64 * a : 64 * a + 32, 128 * j : 128 * j + 128]
-                        two = state[64 * a + 32 : 64 * a + 64, 128 * j : 128 * j + 128]
+                        lanes = pl.ds(128 * j, 128)
+                        one = held[e, g, pl.ds(64 * a, 32), lanes]
+                        two = held[e, g, pl.ds(64 * a + 32, 32), lanes]
                         first = jnp.where(half, one, pltpu.roll(two, 64, 1))
                         second = jnp.where(half, pltpu.roll(one, 64, 1), two)
                         h = 4 * g + 2 * j
@@ -345,11 +349,6 @@
                 sendb[:, k, e, :, pl.ds(a * 128, 128)] = (
                     sbuf[a].reshape(NSP, 8, 128).astype(BF16)
                 )
-        at = jnp.full((1, 512), 2 * sp + k, jnp.int32)
-        pick = jnp.full((1, 512), chosen, jnp.int32)
-        redy[y, k : k + 1, pl.ds(0, 512)] = jnp.where(at <= pick, ybuf[0:1, :], 0.0) + jnp.where(
-            at >= pick, ybuf[1:2, :], 0.0
-        )
         c = pltpu.make_async_copy(sendb.at[sp, k], cache.at[2 * sp + k], own_sem.at[k])
         c.start()
         own_out.append(c)
@@ -360,6 +359,7 @@
     pass_on(2)
     pl.semaphore_wait(stage.at[2], 2)
     states_of(0, pair)
+    arrange(0)
     send_column(0)
     send_states(0, 0, EARLY)
 
@@ -387,56 +387,32 @@
     convolve(TOK - 16, 16)
     states_of(1, pair)
 
-    def y_copy(d, s):
+    def exchange(buffer, me, count, sems, place):
+        for i in range(1, count):
+            other = lax.rem(me + i, count)
+            pltpu.make_async_remote_copy(
+                src_ref=buffer.at[me],
+                dst_ref=buffer.at[me],
+                send_sem=sems.at[0],
+                recv_sem=sems.at[1],
+                device_id=place(other),
+                device_id_type=MESH,
+            ).start()
+
         return pltpu.make_async_remote_copy(
-            src_ref=redy.at[s],
-            dst_ref=redy.at[s],
-            send_sem=ysend.at[d],
-            recv_sem=yrecv.at[s],
-            device_id=at_y(d),
-            device_id_type=MESH,
-        )
-
-    def z_copy(d, s):
-        return pltpu.make_async_remote_copy(
-            src_ref=redz.at[s],
-            dst_ref=redz.at[s],
-            send_sem=zsend.at[d],
-            recv_sem=zrecv.at[s],
-            device_id={"sp": d * NY + y},
-            device_id_type=MESH,
-        )
-
-    def s_copy(d, s):
-        return pltpu.make_async_remote_copy(
-            src_ref=reds.at[s],
-            dst_ref=reds.at[s],
-            send_sem=ssend.at[d],
-            recv_sem=srecv.at[s],
-            device_id={"tp": d},
-            device_id_type=MESH,
-        )
-
-    def each(copy, me, count, act):
-        def body(i, carry):
-            act(copy, me, (me + i) % count)
-            return carry
-
-        lax.fori_loop(1, count, body, 0)
-
-    def start(copy, me, other):
-        copy(other, me).start()
-
-    def receive(copy, me, other):
-        copy(other, other).wait_recv()
-
-    def leave(copy, me, other):
-        copy(other, me).wait_send()
-
-    each(y_copy, y, NY, start)
+            src_ref=buffer.at[pl.ds(0, count - 1)],
+            dst_ref=buffer.at[pl.ds(0, count - 1)],
+            send_sem=sems.at[0],
+            recv_sem=sems.at[1],
+            device_id=place(me),
+            device_id_type=MESH,
+        )
+
+    y_all = exchange(redy, y, NY, ysems, lambda d: {"sp": z * NY + d})
     send_states(0, EARLY, 7)
+    arrange(1)
     send_column(1)
-    send_states(1, 0, 7)
+    send_states(1, 0, MID)
 
     def spread(rows):
         high = rows.astype(BF16)
@@ -448,7 +424,7 @@
         )
 
     gate = jax.nn.silu(gateb[0].astype(F32))
-    each(y_copy, y, NY, receive)
+    y_all.wait_recv()
     base = 2 * NY * z
     ahead_lane = iota((8, 128), 1) < H
     block_log = jnp.zeros((8, 128), F32)
@@ -476,8 +452,9 @@
         partial = partial + wide_weight[8 * k : 8 * k + 8] * redy[:, k, pl.ds(0, 512)]
     redz[z, :, pl.ds(0, 512)] = jnp.sum(partial, axis=0, keepdims=True)
     redz[z, :, pl.ds(512, 128)] = block_log[0:1]
-    each(z_copy, z, NZ, start)
-    each(z_copy, z, NZ, receive)
+    z_all = exchange(redz, z, NZ, zsems, lambda d: {"sp": d * NY + y})
+    send_states(1, MID, 7)
+    z_all.wait_recv()
     lane = iota((1, 128), 1)
     block_rows = []
     for block in range(NZ):
@@ -499,14 +476,22 @@
     gated = tot8[...] * gate
     squares = jnp.sum(jnp.sum(gated * gated, axis=0, keepdims=True), axis=1, keepdims=True)
     reds[tp] = jnp.broadcast_to(squares, (1, 128))
-    each(s_copy, tp, NTP, start)
-    each(s_copy, tp, NTP, receive)
+    s_all = exchange(reds, tp, NTP, ssems, lambda d: {"tp": d})
+    s_all.wait_recv()
     square_sum = jnp.sum(reds[...], axis=0)[:, :64]
     scale = lax.rsqrt(square_sum / (H * P_SIZE) + EPSILON)
     first_read[0] = (gated * scale * gainb[...]).astype(BF16)
 
-    for c in sent:
-        c.wait_send()
+    for j, (start, count) in enumerate(pieces):
+        sent = slab.at[pl.ds(0, NTP - 1), pl.ds(start, count), :]
+        pltpu.make_async_remote_copy(
+            src_ref=sent,
+            dst_ref=sent,
+            send_sem=gsend.at[j],
+            recv_sem=gsend.at[j],
+            device_id={"tp": partner},
+            device_id_type=MESH,
+        ).wait_send()
 
     @pl.when(sp < NSP - 1)
     def _():
@@ -516,13 +501,22 @@
     def _():
         edge_down().wait_send()
 
-    each(y_copy, y, NY, leave)
-    each(z_copy, z, NZ, leave)
-    each(s_copy, tp, NTP, leave)
-    for k in range(2):
-        each(functools.partial(state_copy, k), sp, NSP, receive)
-        each(functools.partial(state_copy, k), sp, NSP, leave)
-        own_out[k].wait()
+    y_all.wait_send()
+    z_all.wait_send()
+    s_all.wait_send()
+    every = cache.at[pl.ds(0, 2 * NSP - 2)]
+    states = pltpu.make_async_remote_copy(
+        src_ref=every,
+        dst_ref=every,
+        send_sem=asend,
+        recv_sem=arecv,
+        device_id={"sp": sp},
+        device_id_type=MESH,
+    )
+    states.wait_recv()
+    states.wait_send()
+    for c in own_out:
+        c.wait()
 
 
 def per_device(*args):
@@ -544,6 +538,7 @@
             pltpu.VMEM((EDGE + TOK, WC), F32),
             pltpu.VMEM((EDGE + TOK + 8, CC), F32),
             pltpu.VMEM((TOK, CC), BF16),
+            pltpu.VMEM((2, 2, N, 256), F32),
             pltpu.VMEM((2, H), F32),
             pltpu.VMEM((2, H), F32),
             pltpu.VMEM((KW, XC), BF16),
@@ -562,18 +557,15 @@
             pltpu.VMEM((8, P_SIZE), F32),
             dma,
             dma((11,)),
-            dma((7, 3)),
+            dma((3,)),
             dma((NTP, 3)),
             dma((2,)),
             dma((2,)),
-            dma((2, NSP)),
-            dma((2, NSP)),
-            dma((NY,)),
-            dma((NY,)),
-            dma((NZ,)),
-            dma((NZ,)),
-            dma((NTP,)),
-            dma((NTP,)),
+            dma,
+            dma,
+            dma((2,)),
+            dma((2,)),
+            dma((2,)),
             dma((2,)),
             pltpu.SemaphoreType.REGULAR((3,)),
         ],

time: 45.4 us -> 42 us (0.925)
  Pallas kernels: 42.6 us -> 39.2 us
    pallas_call x1, Pallas kernels: 42.6 us -> 39.2 us  [per_device(): pl.pallas_call(kernel, out_shape=tuple((pltpu.VMEM(t.shape, t.dtype) for...]
where the time goes in v4:
time: 42 us; the launch traced here: 41.9 us
  Pallas kernels  39.2 us (93%)
  local copies, waits for them, and re-layouts  1.37 us (3%)
  between operations  1.29 us (3%)
    pallas_call x1, Pallas kernels, per_device(): pl.pallas_call(kernel, out_shape=tuple((pltpu.VMEM(t.shape, t.dtype) for...  39.2 us
    unnamed x2, local copies, waits for them, and re-layouts  1.37 us

profile of v4, /device:TPU:1, one launch (start us, length us, event | category | flops | bytes accessed | tf_op | source)
XLA Modules:
  0.0 41.9 jit_solution(12106355360194432574)
XLA Ops:
  1.3 39.2 %shard_map.131 = (bf16[64,2,8,256]{3,2,1,0:T(8,128)(2,1)S(1)}, bf16[1,8,64]{2,1,0:T(8,128)(2,1)S(1)}) custom-call(bf16[256,256]{1,0:T(8,128)(2,1)} %inputs.1, bf16[2048,512]{1,0:T(8,128)(2,1)} %x_weight.1, bf16[2048,256]{1,0:T(8,128)(2,1)} %b_weight.1, bf16[2048,128]{1,0:T(8,128)(2,1)} %dt_weight.1, f32[2,64]{1,0:T(2,128)} %dt_bias.1, f32[2,64]{1,0:T(2,128)} %decay_rate.1, ...), custom_call_target="tpu_custom_call" | custom-call | tf_op jit(solution)/shard_map/pallas_call | solution.py:530
  40.5 0.8 %copy.16 = bf16[64,2,8,256]{3,2,1,0:T(8,128)(2,1)} copy(bf16[64,2,8,256]{3,2,1,0:T(8,128)(2,1)S(1)} %get-tuple-element.2) | data formatting | bytes 1048576
  41.3 0.6 %copy.17 = bf16[1,8,64]{2,1,0:T(8,128)(2,1)} copy(bf16[1,8,64]{2,1,0:T(8,128)(2,1)S(1)} %get-tuple-element.3) | data formatting | bytes 2048

commit v5 on v4

--- a/solution.py
+++ b/solution.py
@@ -28,7 +28,7 @@
 ROWS_A = 144
 ROWS_B = TOK - ROWS_A
 TOP = EDGE + ROWS_A
-EARLY = 3
+EARLY = 2
 MID = 0
 
 MESH = pl.DeviceIdType.MESH
@@ -51,14 +51,13 @@
 ):
     sp = lax.axis_index("sp")
     tp = lax.axis_index("tp")
-    y = sp % NY
-    z = sp // NY
-    x = tp // 2
-    core = tp % 2
-    partner = 2 * x + 1 - core
-    right = 2 * ((x + 1) % NX) + core
-    left = 2 * ((x + NX - 1) % NX) + core
-    across = 2 * ((x + 2) % NX) + core
+    y = lax.rem(sp, NY)
+    z = lax.div(sp, NY)
+    core = lax.rem(tp, 2)
+    partner = tp + 1 - 2 * core
+    right = lax.rem(tp + 2, NTP)
+    left = lax.rem(tp + NTP - 2, NTP)
+    across = lax.rem(tp + NTP // 2, NTP)
 
     own_in = pltpu.make_async_copy(inputs, slab.at[tp, pl.ds(EDGE, TOK), :], in_sem)
     own_in.start()
@@ -84,30 +83,25 @@
     barrier = pltpu.get_barrier_semaphore()
 
     def at_y(other):
-        return {"sp": z * NY + (other + NY) % NY}
-
-    def greet_tp(i, carry):
+        return {"sp": z * NY + lax.rem(other, NY)}
+
+    for i in range(1, NTP):
         pl.semaphore_signal(
-            barrier, inc=1, device_id={"tp": (tp + i) % NTP}, device_id_type=MESH
-        )
-        return carry
-
-    def greet_z(i, carry):
+            barrier, inc=1, device_id={"tp": lax.rem(tp + i, NTP)}, device_id_type=MESH
+        )
+    for i in range(1, NZ):
         pl.semaphore_signal(
-            barrier, inc=1, device_id={"sp": ((z + i) % NZ) * NY + y}, device_id_type=MESH
-        )
-        return carry
-
-    lax.fori_loop(1, NTP, greet_tp, 0)
-    lax.fori_loop(1, NZ, greet_z, 0)
-    for side in (1, -1):
+            barrier, inc=1, device_id={"sp": lax.rem(z + i, NZ) * NY + y}, device_id_type=MESH
+        )
+    for side in (1, NY - 1):
         pl.semaphore_signal(barrier, inc=1, device_id=at_y(y + side), device_id_type=MESH)
+    for side in (1, NSP - 1):
         pl.semaphore_signal(
-            barrier, inc=1, device_id={"sp": (sp + NSP + side) % NSP}, device_id_type=MESH
+            barrier, inc=1, device_id={"sp": lax.rem(sp + side, NSP)}, device_id_type=MESH
         )
 
     def tell(index, distance):
-        for side in (distance, -distance):
+        for side in (distance, NY - distance):
             pl.semaphore_signal(
                 stage.at[index], inc=1, device_id=at_y(y + side), device_id_type=MESH
             )
@@ -126,7 +120,7 @@
             dst_ref=slab.at[tp, pl.ds(0, EDGE), :],
             send_sem=hsend.at[0],
             recv_sem=hrecv.at[0],
-            device_id={"sp": (sp + 1) % NSP},
+            device_id={"sp": lax.rem(sp + 1, NSP)},
             device_id_type=MESH,
         )
 
@@ -231,7 +225,7 @@
             dst_ref=proj.at[pl.ds(EDGE + TOK, 8), :],
             send_sem=hsend.at[1],
             recv_sem=hrecv.at[1],
-            device_id={"sp": (sp + NSP - 1) % NSP},
+            device_id={"sp": lax.rem(sp + NSP - 1, NSP)},
             device_id_type=MESH,
         )
 
@@ -519,6 +513,20 @@
         c.wait()
 
 
+def write_out(cache, first_read, cache_out, first_out, sems):
+    copies = [
+        pltpu.make_async_copy(
+            cache.at[pl.ds(16 * i, 16)], cache_out.at[pl.ds(16 * i, 16)], sems.at[i]
+        )
+        for i in range(4)
+    ]
+    copies.append(pltpu.make_async_copy(first_read, first_out, sems.at[4]))
+    for c in copies:
+        c.start()
+    for c in copies:
+        c.wait()
+
+
 def per_device(*args):
     dma = pltpu.SemaphoreType.DMA
     any_spec = pl.BlockSpec(memory_space=pl.ANY)
@@ -527,7 +535,7 @@
         jax.ShapeDtypeStruct((64, 2, 8, 256), BF16),
         jax.ShapeDtypeStruct((1, 8, 64), BF16),
     )
-    return pl.pallas_call(
+    results = pl.pallas_call(
         kernel,
         out_shape=tuple(pltpu.VMEM(t.shape, t.dtype) for t in shapes),
         in_specs=[any_spec] * 12,
@@ -571,6 +579,14 @@
         ],
         compiler_params=pltpu.CompilerParams(collective_id=0, has_side_effects=True),
     )(*args)
+    results = [pltpu.with_memory_space_constraint(r, pltpu.VMEM) for r in results]
+    return pl.pallas_call(
+        write_out,
+        out_shape=shapes,
+        in_specs=[vmem_spec] * 2,
+        out_specs=(any_spec, any_spec),
+        scratch_shapes=[dma((5,))],
+    )(*results)
 
 
 def solution(mesh):

time: 42 us -> 40.7 us (0.969)
  local copies, waits for them, and re-layouts: 1.37 us -> 0 us
    unnamed x2 -> x0, local copies, waits for them, and re-layouts: 1.37 us -> none
    pallas_call x0 -> x1, Pallas kernels: none -> 0.83 us  [per_device(): pl.pallas_call(write_out, out_shape=shapes, in_specs=[vmem_spec] * 2, out...]
    pallas_call x1, Pallas kernels: 39.2 us -> 38.4 us  [per_device(): pl.pallas_call(kernel, out_shape=tuple((pltpu.VMEM(t.shape, t.dtype) for...]
where the time goes in v5:
time: 40.7 us; the launch traced here: 40.6 us
  Pallas kernels  39.3 us (97%)
  between operations  1.29 us (3%)
    pallas_call x1, Pallas kernels, per_device(): pl.pallas_call(kernel, out_shape=tuple((pltpu.VMEM(t.shape, t.dtype) for...  38.4 us
    pallas_call x1, Pallas kernels, per_device(): pl.pallas_call(write_out, out_shape=shapes, in_specs=[vmem_spec] * 2, out...  0.83 us

profile of v5, /device:TPU:1, one launch (start us, length us, event | category | flops | bytes accessed | tf_op | source)
XLA Modules:
  0.0 40.6 jit_solution(9740477367222975108)
XLA Ops:
  1.3 38.4 %shard_map.131 = (bf16[64,2,8,256]{3,2,1,0:T(8,128)(2,1)S(1)}, bf16[1,8,64]{2,1,0:T(8,128)(2,1)S(1)}) custom-call(bf16[256,256]{1,0:T(8,128)(2,1)} %inputs.1, bf16[2048,512]{1,0:T(8,128)(2,1)} %x_weight.1, bf16[2048,256]{1,0:T(8,128)(2,1)} %b_weight.1, bf16[2048,128]{1,0:T(8,128)(2,1)} %dt_weight.1, f32[2,64]{1,0:T(2,128)} %dt_bias.1, f32[2,64]{1,0:T(2,128)} %decay_rate.1, ...), custom_call_target="tpu_custom_call" | custom-call | tf_op jit(solution)/shard_map/pallas_call | solution.py:538
  39.7 0.8 %shard_map.132 = (bf16[64,2,8,256]{3,2,1,0:T(8,128)(2,1)}, bf16[1,8,64]{2,1,0:T(8,128)(2,1)}) custom-call(bf16[64,2,8,256]{3,2,1,0:T(8,128)(2,1)S(1)} %get-tuple-element.4.cache, bf16[1,8,64]{2,1,0:T(8,128)(2,1)S(1)} %get-tuple-element.5.first_read), custom_call_target="tpu_custom_call" | custom-call | tf_op jit(solution)/shard_map/pallas_call | solution.py:583

commit v6 on v5

--- a/solution.py
+++ b/solution.py
@@ -61,10 +61,14 @@
 
     own_in = pltpu.make_async_copy(inputs, slab.at[tp, pl.ds(EDGE, TOK), :], in_sem)
     own_in.start()
-    loads = [
-        (x_weight, wbuf.at[:, pl.ds(0, XC)]),
-        (b_weight, wbuf.at[:, pl.ds(XC, BC)]),
-        (dt_weight, wbuf.at[:, pl.ds(CC, 128)]),
+    loads = []
+    for width, weight, first, cuts in (
+        (XC, x_weight, 0, 4), (BC, b_weight, XC, 2), (128, dt_weight, CC, 1)
+    ):
+        for i in range(cuts):
+            depth = pl.ds(i * (2048 // cuts), 2048 // cuts)
+            loads.append((weight.at[depth, :], wbuf.at[depth, pl.ds(first, width)]))
+    loads += [
         (dt_bias, biasb),
         (decay_rate, rateb),
         (conv_x, cxb),
@@ -77,7 +81,7 @@
     copies = []
     for i, (src, dst) in enumerate(loads):
         c = pltpu.make_async_copy(src, dst, load_sems.at[i])
-        c.start()
+        c.start(priority=1)
         copies.append(c)
 
     barrier = pltpu.get_barrier_semaphore()
@@ -564,7 +568,7 @@
             pltpu.VMEM((NTP, 1, 128), F32),
             pltpu.VMEM((8, P_SIZE), F32),
             dma,
-            dma((11,)),
+            dma((15,)),
             dma((3,)),
             dma((NTP, 3)),
             dma((2,)),

time: 40.7 us -> 40.7 us (level)
  no operation moved by 1% of the time
where the time goes in v6:
time: 40.7 us; the launch traced here: 40.5 us
  Pallas kernels  39.2 us (96%)
  between operations  1.29 us (3%)
    pallas_call x1, Pallas kernels, per_device(): pl.pallas_call(kernel, out_shape=tuple((pltpu.VMEM(t.shape, t.dtype) for...  38.4 us
    pallas_call x1, Pallas kernels, per_device(): pl.pallas_call(write_out, out_shape=shapes, in_specs=[vmem_spec] * 2, out...  0.83 us

profile of v6, /device:TPU:1, one launch (start us, length us, event | category | flops | bytes accessed | tf_op | source)
XLA Modules:
  0.0 40.5 jit_solution(6282558515619131458)
XLA Ops:
  1.3 38.4 %shard_map.131 = (bf16[64,2,8,256]{3,2,1,0:T(8,128)(2,1)S(1)}, bf16[1,8,64]{2,1,0:T(8,128)(2,1)S(1)}) custom-call(bf16[256,256]{1,0:T(8,128)(2,1)} %inputs.1, bf16[2048,512]{1,0:T(8,128)(2,1)} %x_weight.1, bf16[2048,256]{1,0:T(8,128)(2,1)} %b_weight.1, bf16[2048,128]{1,0:T(8,128)(2,1)} %dt_weight.1, f32[2,64]{1,0:T(2,128)} %dt_bias.1, f32[2,64]{1,0:T(2,128)} %decay_rate.1, ...), custom_call_target="tpu_custom_call" | custom-call | tf_op jit(solution)/shard_map/pallas_call | solution.py:542
  39.7 0.8 %shard_map.132 = (bf16[64,2,8,256]{3,2,1,0:T(8,128)(2,1)}, bf16[1,8,64]{2,1,0:T(8,128)(2,1)}) custom-call(bf16[64,2,8,256]{3,2,1,0:T(8,128)(2,1)S(1)} %get-tuple-element.4.cache, bf16[1,8,64]{2,1,0:T(8,128)(2,1)S(1)} %get-tuple-element.5.first_read), custom_call_target="tpu_custom_call" | custom-call | tf_op jit(solution)/shard_map/pallas_call | solution.py:587

commit v7 on v6

--- a/solution.py
+++ b/solution.py
@@ -321,9 +321,14 @@
                 state = jnp.dot(
                     keys_t[g], weighted[:, g * 256 : (g + 1) * 256], preferred_element_type=F32
                 )
-                read = jnp.dot(queries[g], state.astype(BF16), preferred_element_type=F32)
+                held[e, g] = state
+    def read_of(k):
+        for e in range(2):
+            for g in range(2):
+                read = jnp.dot(
+                    queries[g], held[e, g].astype(BF16), preferred_element_type=F32
+                )
                 ybuf[e : e + 1, pl.ds(g * 256, 256)] = read[0:1]
-                held[e, g] = state
         at = jnp.full((1, 512), 2 * sp + k, jnp.int32)
         pick = jnp.full((1, 512), chosen, jnp.int32)
         redy[y, k : k + 1, pl.ds(0, 512)] = jnp.where(at <= pick, ybuf[0:1, :], 0.0) + jnp.where(
@@ -360,6 +365,7 @@
     arrange(0)
     send_column(0)
     send_states(0, 0, EARLY)
+    read_of(0)
 
     for slot in (partner, *ring, twin(right), twin(left)):
         if slot is not right and slot is not left and slot is not across:
@@ -384,6 +390,7 @@
 
     convolve(TOK - 16, 16)
     states_of(1, pair)
+    read_of(1)
 
     def exchange(buffer, me, count, sems, place):
         for i in range(1, count):

time: 40.7 us -> 40.6 us (level)
  no operation moved by 1% of the time
where the time goes in v7:
time: 40.6 us; the launch traced here: 40.5 us
  Pallas kernels  39.2 us (97%)
  between operations  1.29 us (3%)
    pallas_call x1, Pallas kernels, per_device(): pl.pallas_call(kernel, out_shape=tuple((pltpu.VMEM(t.shape, t.dtype) for...  38.4 us
    pallas_call x1, Pallas kernels, per_device(): pl.pallas_call(write_out, out_shape=shapes, in_specs=[vmem_spec] * 2, out...  0.83 us

profile of v7, /device:TPU:1, one launch (start us, length us, event | category | flops | bytes accessed | tf_op | source)
XLA Modules:
  0.0 40.5 jit_solution(16135484850261416857)
XLA Ops:
  1.3 38.4 %shard_map.131 = (bf16[64,2,8,256]{3,2,1,0:T(8,128)(2,1)S(1)}, bf16[1,8,64]{2,1,0:T(8,128)(2,1)S(1)}) custom-call(bf16[256,256]{1,0:T(8,128)(2,1)} %inputs.1, bf16[2048,512]{1,0:T(8,128)(2,1)} %x_weight.1, bf16[2048,256]{1,0:T(8,128)(2,1)} %b_weight.1, bf16[2048,128]{1,0:T(8,128)(2,1)} %dt_weight.1, f32[2,64]{1,0:T(2,128)} %dt_bias.1, f32[2,64]{1,0:T(2,128)} %decay_rate.1, ...), custom_call_target="tpu_custom_call" | custom-call | tf_op jit(solution)/shard_map/pallas_call | solution.py:549
  39.6 0.8 %shard_map.132 = (bf16[64,2,8,256]{3,2,1,0:T(8,128)(2,1)}, bf16[1,8,64]{2,1,0:T(8,128)(2,1)}) custom-call(bf16[64,2,8,256]{3,2,1,0:T(8,128)(2,1)S(1)} %get-tuple-element.4.cache, bf16[1,8,64]{2,1,0:T(8,128)(2,1)S(1)} %get-tuple-element.5.first_read), custom_call_target="tpu_custom_call" | custom-call | tf_op jit(solution)/shard_map/pallas_call | solution.py:594

commit v8 on v6

--- a/solution.py
+++ b/solution.py
@@ -165,7 +165,7 @@
     ring = (right, left, across)
 
     def pass_on(j):
-        for slot in ring:
+        for slot in (across, right, left):
             arrive(slot, j)
             forward(slot, j, partner)
 
@@ -196,14 +196,14 @@
     send_own(2)
     for c in copies:
         c.wait()
+    acc[pl.ds(0, TOP), :] = product(tp, 0, TOP)
+    pass_on(0)
+    pl.semaphore_wait(stage.at[0], 2)
+    tell(1, 2)
     acc[pl.ds(TOP, ROWS_B), :] = product(tp, TOP, ROWS_B)
-    acc[pl.ds(0, TOP), :] = product(tp, 0, TOP)
     for j in (0, 1):
         arrive(partner, j)
     add(partner, 0, TOP)
-    pass_on(0)
-    pl.semaphore_wait(stage.at[0], 2)
-    tell(1, 2)
     pass_on(1)
     for slot in ring:
         add(slot, 0, TOP)

time: 40.7 us -> 40.6 us (level)
  no operation moved by 1% of the time
where the time goes in v8:
time: 40.6 us; the launch traced here: 40.5 us
  Pallas kernels  39.2 us (97%)
  between operations  1.29 us (3%)
    pallas_call x1, Pallas kernels, per_device(): pl.pallas_call(kernel, out_shape=tuple((pltpu.VMEM(t.shape, t.dtype) for...  38.4 us
    pallas_call x1, Pallas kernels, per_device(): pl.pallas_call(write_out, out_shape=shapes, in_specs=[vmem_spec] * 2, out...  0.83 us

profile of v8, /device:TPU:1, one launch (start us, length us, event | category | flops | bytes accessed | tf_op | source)
XLA Modules:
  0.0 40.5 jit_solution(9925193529412106922)
XLA Ops:
  1.3 38.4 %shard_map.131 = (bf16[64,2,8,256]{3,2,1,0:T(8,128)(2,1)S(1)}, bf16[1,8,64]{2,1,0:T(8,128)(2,1)S(1)}) custom-call(bf16[256,256]{1,0:T(8,128)(2,1)} %inputs.1, bf16[2048,512]{1,0:T(8,128)(2,1)} %x_weight.1, bf16[2048,256]{1,0:T(8,128)(2,1)} %b_weight.1, bf16[2048,128]{1,0:T(8,128)(2,1)} %dt_weight.1, f32[2,64]{1,0:T(2,128)} %dt_bias.1, f32[2,64]{1,0:T(2,128)} %decay_rate.1, ...), custom_call_target="tpu_custom_call" | custom-call | tf_op jit(solution)/shard_map/pallas_call | solution.py:542
  39.7 0.8 %shard_map.132 = (bf16[64,2,8,256]{3,2,1,0:T(8,128)(2,1)}, bf16[1,8,64]{2,1,0:T(8,128)(2,1)}) custom-call(bf16[64,2,8,256]{3,2,1,0:T(8,128)(2,1)S(1)} %get-tuple-element.4.cache, bf16[1,8,64]{2,1,0:T(8,128)(2,1)S(1)} %get-tuple-element.5.first_read), custom_call_target="tpu_custom_call" | custom-call | tf_op jit(solution)/shard_map/pallas_call | solution.py:587
